TPU v7x, 32 devices: a whole 2x2x4 slice. The times are simulated.
32 devices in a mesh: ep: 8 (over z, x), tp: 4 (over y, core).
Axes of the slice: x: 2, y: 2, z: 4, core: 2. Of those that a mesh axis runs over, the one named last changes fastest.
Arguments:
- pool_input: bfloat16 [4096, 1024], P('ep', 'tp'), may hold values from -6 to 6
- group_weight: bfloat16 [4, 256, 256], P('tp'), may hold values from -0.375 to 0.375
- pool_scale: float32 [1024], P('tp'), may hold values from 0.1 to 1.9
- out_weight: bfloat16 [1024, 2048], P('tp'), may hold values from -0.1875 to 0.1875
- mix_gain: float32 [2048], replicated, may hold values from 0.1 to 1.9
- expert_input: bfloat16 [8192, 2048], P(('ep', 'tp')), may hold values from -6 to 6
- routes: int32 [8192, 2], P('ep'), may hold values from 0 to 15, all different within a row; in each aligned block of 256 rows (0 to 255, 256 to 511, ...) at most 40 rows name the same one
- route_weights: float32 [8192, 2], P('ep'), may hold values from 0.2 to 2.5
- moe_in_gain: float32 [2048], replicated, may hold values from 0.1 to 1.9
- gate_weight: bfloat16 [16, 2048, 1024], P('ep', None, 'tp'), may hold values from -0.125 to 0.125
- up_weight: bfloat16 [16, 2048, 1024], P('ep', None, 'tp'), may hold values from -0.125 to 0.125
- down_weight: bfloat16 [16, 1024, 2048], P('ep', 'tp'), may hold values from -0.1875 to 0.1875
- moe_out_gain: float32 [2048], replicated, may hold values from 0.1 to 1.9
Outputs:
- mixer_out: bfloat16 [4096, 2048], P(('ep', 'tp'))
- moe_out: bfloat16 [8192, 2048], P(('ep', 'tp'))
Inputs may be any that keep to these rules, and one draw needn't show every extreme that they name: `routes`: each row names 2 different experts. In each aligned block of 256 rows no expert is named by more than 40 rows, a bound that some block reaches.
All inputs are finite; a program needn't handle non-finite values.
Results may differ from a plain program's by a relative error of at most 0.013.
Values may be sent and summed in bfloat16 or wider, within the bound.
A program may use at most 128 MiB of HBM per device.

v0:
```python
import functools

import jax
import jax.numpy as jnp
from jax import lax
from jax.experimental import pallas as pl
from jax.experimental.pallas import tpu as pltpu
from jax.sharding import PartitionSpec as P

NORM_EPS = 1e-06


def passed_along(value, axis, steps):
    count = lax.axis_size(axis)
    initial, last = (max(0, -steps), min(count, count - steps))
    return lax.ppermute(value, axis, [(source, source + steps) for source in range(initial, last)])


def rms_scale(values, gain_vec):
    mean_sq = jnp.mean(values * values, axis=-1, keepdims=True)
    return values * lax.rsqrt(mean_sq + NORM_EPS) * gain_vec


def slot_numbers(route_block, experts, capacity, exp_dev, block_rows):
    flat_routes = route_block.reshape(-1)
    one_hot = (flat_routes[:, None] == jnp.arange(experts, dtype=jnp.int32)[None, :]).astype(
        jnp.int32
    )
    slot_rank = jnp.sum((jnp.cumsum(one_hot, axis=0) - one_hot) * one_hot, axis=1)
    owner = flat_routes // exp_dev
    local = flat_routes - owner * exp_dev
    return owner * block_rows + local * capacity + slot_rank


MESH = pl.DeviceIdType.MESH


def exchange_kernel(
    capacity,
    outgoing,
    mix_part,
    gate_hbm,
    up_hbm,
    down_hbm,
    returned,
    projected,
    arrived,
    part,
    core_in,
    chip_sum,
    cross_in,
    final,
    gate,
    up,
    down,
    mix_held,
    mix_core,
    mix_sum,
    mix_cross,
    local_sem,
    dis_send,
    dis_recv,
    y1_send,
    y1_recv,
    c1_send,
    c1_recv,
    c2_send,
    c2_recv,
    y2_send,
    y2_recv,
    ret_send,
    ret_recv,
    m1_send,
    m1_recv,
    m2_send,
    m2_recv,
):
    ep_size, tp_size, rows, width = arrived.shape
    exp_dev, _, ff_dev = gate.shape
    highs = tp_size // 2
    ep = lax.axis_index("ep")
    tp = lax.axis_index("tp")
    hi, lo = tp // 2, tp % 2
    other = 1 - lo

    def remote(src, dst, send, recv, to_ep, to_tp):
        return pltpu.make_async_remote_copy(
            src_ref=src,
            dst_ref=dst,
            send_sem=send,
            recv_sem=recv,
            device_id=(to_ep, to_tp),
            device_id_type=MESH,
        )

    def peer_high(k):
        return lax.rem(hi + k, highs)

    def offset_of(i):
        far = jnp.where(i < 2, 2 * i + 1, ep_size + 1 - i)
        return jnp.where(i < ep_size - 2, far, 2 * (ep_size - 1 - i))

    def partner_ep(d):
        low = d
        mine = ep
        value = ep * 0
        bit = 1
        while bit < ep_size:
            a = (mine // bit) % 2
            b = (low // bit) % 2
            value = value + bit * ((a + b) % 2)
            bit *= 2
        return value

    def dispatch(d):
        peer = partner_ep(d)
        return remote(
            outgoing.at[peer], arrived.at[d, tp], dis_send.at[d], dis_recv.at[d], peer, tp
        )

    def gather_cross(d, k):
        high = peer_high(k)
        return remote(
            arrived.at[d, tp],
            arrived.at[d, tp],
            y1_send.at[d, k],
            y1_recv.at[d, highs - k],
            ep,
            high * 2 + lo,
        )

    def gather_cross_in(d, k):
        high = peer_high(k)
        return remote(
            arrived.at[d, high * 2 + lo],
            arrived.at[d, high * 2 + lo],
            y1_send.at[d, k],
            y1_recv.at[d, k],
            ep,
            high * 2 + lo,
        )

    def gather_core(d, high):
        slot = arrived.at[d, high * 2 + lo]
        return remote(slot, slot, c1_send.at[d, high], c1_recv.at[d, high], ep, hi * 2 + other)

    def gather_core_in(d, high):
        slot = arrived.at[d, high * 2 + other]
        return remote(slot, slot, c1_send.at[d, high], c1_recv.at[d, high], ep, hi * 2 + other)

    def reduce_core(d, high):
        return remote(
            part.at[high * 2 + other],
            core_in.at[d, high],
            c2_send.at[d, high],
            c2_recv.at[d, high],
            ep,
            hi * 2 + other,
        )

    def reduce_cross(d, k):
        high = peer_high(k)
        return remote(
            chip_sum.at[high],
            cross_in.at[d, highs - k - 1],
            y2_send.at[d, k],
            y2_recv.at[d, highs - k],
            ep,
            high * 2 + lo,
        )

    def reduce_cross_in(d, k):
        high = peer_high(k)
        return remote(
            chip_sum.at[high],
            cross_in.at[d, k - 1],
            y2_send.at[d, k],
            y2_recv.at[d, k],
            ep,
            high * 2 + lo,
        )

    def give_back(d):
        peer = partner_ep(d)
        return remote(final.at[d], returned.at[ep], ret_send.at[d], ret_recv.at[d], peer, tp)

    def give_back_in(d):
        peer = partner_ep(d)
        return remote(final.at[d], returned.at[peer], ret_send.at[d], ret_recv.at[d], peer, tp)

    def mix_core_copy(high):
        return remote(
            mix_held.at[high * 2 + other],
            mix_core.at[high],
            m1_send.at[high],
            m1_recv.at[high],
            ep,
            hi * 2 + other,
        )

    def mix_cross_copy(k):
        high = peer_high(k)
        return remote(
            mix_sum.at[high],
            mix_cross.at[highs - k - 1],
            m2_send.at[k],
            m2_recv.at[highs - k],
            ep,
            high * 2 + lo,
        )

    def mix_cross_in(k):
        high = peer_high(k)
        return remote(
            mix_sum.at[high],
            mix_cross.at[k - 1],
            m2_send.at[k],
            m2_recv.at[k],
            ep,
            high * 2 + lo,
        )

    own_rows = pltpu.make_async_copy(outgoing.at[ep], arrived.at[0, tp], local_sem.at[0])
    own_mix = pltpu.make_async_copy(mix_part, mix_held, local_sem.at[1])
    weight_copies = [
        pltpu.make_async_copy(gate_hbm, gate, local_sem.at[2]),
        pltpu.make_async_copy(up_hbm, up, local_sem.at[3]),
        pltpu.make_async_copy(down_hbm, down, local_sem.at[4]),
    ]
    own_rows.start()
    own_mix.start()
    for copy in weight_copies:
        copy.start()

    barrier = pltpu.get_barrier_semaphore()

    def greet(d, carry):
        pl.semaphore_signal(barrier, inc=1, device_id=(partner_ep(d), tp), device_id_type=MESH)
        return carry

    lax.fori_loop(1, ep_size, greet, 0)
    for k in range(1, highs):
        pl.semaphore_signal(
            barrier, inc=1, device_id=(ep, peer_high(k) * 2 + lo), device_id_type=MESH
        )
    pl.semaphore_signal(barrier, inc=1, device_id=(ep, hi * 2 + other), device_id_type=MESH)
    pl.semaphore_wait(barrier, ep_size - 1 + highs)

    def send_out(i, carry):
        dispatch(offset_of(i)).start()
        return carry

    lax.fori_loop(0, ep_size - 1, send_out, 0)

    def stage_a(d):
        for k in range(1, highs):
            gather_cross(d, k).start()
        gather_core(d, hi).start()

    own_rows.wait()
    stage_a(0)

    own_mix.wait()
    for high in range(highs):
        mix_core_copy(high).start()
    for high in range(highs):
        mix_core_copy(high).wait_recv()
    for high in range(highs):
        mix_sum[high] = (
            mix_held[high * 2 + lo].astype(jnp.float32) + mix_core[high].astype(jnp.float32)
        ).astype(jnp.bfloat16)
    for k in range(1, highs):
        mix_cross_copy(k).start()
    first = offset_of(ep * 0)
    dispatch(first).wait_recv()
    stage_a(first)
    for copy in weight_copies:
        copy.wait()

    row_expert = (
        lax.rem(lax.broadcasted_iota(jnp.int32, (tp_size * rows, 1), 0), rows) // capacity
    )
    column_step = min(width, 512)

    def step(i, carry):
        @pl.when(i + 1 < ep_size - 1)
        def _():
            d = offset_of(i + 1)
            dispatch(d).wait_recv()
            stage_a(d)

        @pl.when(i < ep_size)
        def _():
            d = offset_of(i)
            for k in range(1, highs):
                gather_cross_in(d, k).wait_recv()
                gather_core(d, peer_high(k)).start()

        @pl.when(i >= 2)
        def _():
            d = offset_of(i - 2)
            total = chip_sum[hi].astype(jnp.float32)
            for k in range(1, highs):
                reduce_cross(d, k).wait_send()
                reduce_cross_in(d, k).wait_recv()
                total = total + cross_in[d, k - 1].astype(jnp.float32)
            final[d] = total.astype(jnp.bfloat16)

            @pl.when(i == ep_size + 1)
            def _():
                pltpu.make_async_copy(final.at[0], returned.at[ep], local_sem.at[0]).start()

            @pl.when(i <= ep_size)
            def _():
                give_back(d).start()

        @pl.when((i >= 1) & (i <= ep_size))
        def _():
            d = offset_of(i - 1)
            for high in range(highs):
                reduce_core(d, high).wait_recv()
                reduce_core(d, high).wait_send()
                chip_sum[high] = (
                    part[high * 2 + lo].astype(jnp.float32) + core_in[d, high].astype(jnp.float32)
                ).astype(jnp.bfloat16)
            for k in range(1, highs):
                reduce_cross(d, k).start()

        @pl.when(i < ep_size)
        def _():
            d = offset_of(i)
            for high in range(highs):
                gather_core_in(d, high).wait_recv()
            hidden = []
            for e in range(exp_dev):
                block = arrived[d].reshape(tp_size * rows, width)
                gate_act = jnp.dot(block, gate[e], preferred_element_type=jnp.float32)
                up_act = jnp.dot(block, up[e], preferred_element_type=jnp.float32)
                act = gate_act / (1.0 + jnp.exp(-gate_act)) * up_act
                hidden.append(jnp.where(row_expert == e, act, 0.0).astype(jnp.bfloat16))
            joined = jnp.concatenate(hidden, axis=1)
            for start in range(0, width, column_step):
                columns = slice(start, start + column_step)
                out = jnp.dot(
                    joined,
                    down[:, :, columns].reshape(exp_dev * ff_dev, column_step),
                    preferred_element_type=jnp.float32,
                )
                part[:, :, columns] = out.astype(jnp.bfloat16).reshape(tp_size, rows, column_step)
            for high in range(highs):
                reduce_core(d, high).start()

        return carry

    lax.fori_loop(0, ep_size + 2, step, 0)

    total = mix_sum[hi].astype(jnp.float32)
    for k in range(1, highs):
        mix_cross_in(k).wait_recv()
        total = total + mix_cross[k - 1].astype(jnp.float32)
    projected[...] = total
    for k in range(1, highs):
        mix_cross_copy(k).wait_send()
    for high in range(highs):
        mix_core_copy(high).wait_send()

    def drain_all(d, carry):
        for k in range(1, highs):
            gather_cross(d, k).wait_send()
        for high in range(highs):
            gather_core(d, high).wait_send()
        return carry

    lax.fori_loop(0, ep_size, drain_all, 0)

    def drain(i, carry):
        d = offset_of(i)
        dispatch(d).wait_send()
        give_back(d).wait_send()
        give_back_in(d).wait_recv()
        return carry

    lax.fori_loop(0, ep_size - 1, drain, 0)
    pltpu.make_async_copy(final.at[0], returned.at[ep], local_sem.at[0]).wait()


def exchange(outgoing, mix_part, gate_weight, up_weight, down_weight, capacity):
    ep_size, rows, width = outgoing.shape
    tp_size, mix_rows, _ = mix_part.shape
    highs = tp_size // 2
    bf16 = jnp.bfloat16
    any_spec = pl.BlockSpec(memory_space=pl.ANY)
    dma = pltpu.SemaphoreType.DMA
    pair = (ep_size, highs)
    flops = 6 * gate_weight.size * ep_size * tp_size * rows
    return pl.pallas_call(
        functools.partial(exchange_kernel, capacity),
        out_shape=(
            jax.ShapeDtypeStruct(outgoing.shape, bf16),
            jax.ShapeDtypeStruct((mix_rows, width), jnp.float32),
        ),
        in_specs=[any_spec] * 5,
        out_specs=(any_spec, pl.BlockSpec(memory_space=pltpu.VMEM)),
        scratch_shapes=[
            pltpu.VMEM((ep_size, tp_size, rows, width), bf16),
            pltpu.VMEM((tp_size, rows, width), bf16),
            pltpu.VMEM((ep_size, highs, rows, width), bf16),
            pltpu.VMEM((highs, rows, width), bf16),
            pltpu.VMEM((ep_size, highs - 1, rows, width), bf16),
            pltpu.VMEM((ep_size, rows, width), bf16),
            pltpu.VMEM(gate_weight.shape, bf16),
            pltpu.VMEM(up_weight.shape, bf16),
            pltpu.VMEM(down_weight.shape, bf16),
            pltpu.VMEM(mix_part.shape, bf16),
            pltpu.VMEM((highs, mix_rows, width), bf16),
            pltpu.VMEM((highs, mix_rows, width), bf16),
            pltpu.VMEM((highs - 1, mix_rows, width), bf16),
            dma((5,)),
            dma((ep_size,)),
            dma((ep_size,)),
            dma(pair),
            dma(pair),
            dma(pair),
            dma(pair),
            dma(pair),
            dma(pair),
            dma(pair),
            dma(pair),
            dma((ep_size,)),
            dma((ep_size,)),
            dma((highs,)),
            dma((highs,)),
            dma((highs,)),
            dma((highs,)),
        ],
        compiler_params=pltpu.CompilerParams(
            collective_id=0, has_side_effects=True, vmem_limit_bytes=60 * 1024 * 1024
        ),
        cost_estimate=pl.CostEstimate(
            flops=flops, bytes_accessed=4 * outgoing.size, transcendentals=0
        ),
    )(outgoing, mix_part, gate_weight, up_weight, down_weight)


def on_device(
    pool_input,
    group_weight,
    pool_scale,
    out_weight,
    mix_gain,
    expert_input,
    routes,
    route_weights,
    moe_in_gain,
    gate_weight,
    up_weight,
    down_weight,
    moe_out_gain,
):
    tp_size = lax.axis_size("tp")
    ep_size = lax.axis_size("ep")
    tp_index = lax.axis_index("tp")
    rows_a = pool_input.shape[0]
    model_width = out_weight.shape[1]
    history_rows = 2**tp_size
    window = jnp.left_shift(jnp.int32(2), tp_index)
    history = passed_along(pool_input[rows_a - history_rows :], "ep", 1)
    extended = jnp.concatenate([history, pool_input], axis=0).astype(jnp.float32)
    running = jnp.cumsum(extended, axis=0)
    lagged = lax.dynamic_slice_in_dim(running, history_rows - window, rows_a, 0)
    current = running[history_rows:]
    position = lax.axis_index("ep") * rows_a + jnp.arange(rows_a, dtype=jnp.int32)
    divisor = jnp.minimum(position + 1, window).astype(jnp.float32)[:, None]
    pooled = ((current - lagged) / divisor - extended[history_rows:]).astype(jnp.bfloat16)
    grouped = (
        jnp.dot(pooled, group_weight[0], preferred_element_type=jnp.float32) * pool_scale
    ).astype(jnp.bfloat16)
    exp_dev = gate_weight.shape[0]
    experts = exp_dev * ep_size
    tok_dev = expert_input.shape[0]
    top_count = routes.shape[1]
    capacity = max(2, 5 * tok_dev * top_count // (4 * experts))
    block_rows = -(-exp_dev * capacity // 16) * 16
    slots_total = ep_size * block_rows
    normed = rms_scale(expert_input.astype(jnp.float32), moe_in_gain).astype(jnp.bfloat16)
    own_routes = lax.dynamic_slice_in_dim(routes, tp_index * tok_dev, tok_dev, 0)
    own_slots = slot_numbers(own_routes, experts, capacity, exp_dev, block_rows)
    slot_pairs = own_slots.reshape(tok_dev, top_count)
    slot_range = jnp.arange(slots_total, dtype=jnp.int32)
    chosen = slot_pairs[:, 0][None, :] == slot_range[:, None]
    for k in range(1, top_count):
        chosen = chosen | (slot_pairs[:, k][None, :] == slot_range[:, None])
    outgoing = (
        jnp.dot(chosen.astype(jnp.bfloat16), normed, preferred_element_type=jnp.float32)
        .astype(jnp.bfloat16)
        .reshape(ep_size, block_rows, model_width)
    )
    mix_part = (
        jnp.dot(grouped, out_weight, preferred_element_type=jnp.float32)
        .astype(jnp.bfloat16)
        .reshape(tp_size, rows_a // tp_size, model_width)
    )
    returned, projected = exchange(
        outgoing, mix_part, gate_weight, up_weight, down_weight, capacity
    )
    mixer_out = rms_scale(projected, mix_gain).astype(jnp.bfloat16)
    back = returned.reshape(slots_total, model_width)
    own_weights = lax.dynamic_slice_in_dim(route_weights, tp_index * tok_dev, tok_dev, 0)
    combined = jnp.zeros((tok_dev, model_width), jnp.float32)
    for k in range(top_count):
        place = (slot_pairs[:, k : k + 1] == slot_range[None, :]).astype(jnp.bfloat16)
        picked = jnp.dot(place, back, preferred_element_type=jnp.float32)
        combined = combined + picked * own_weights[:, k : k + 1]
    moe_out = rms_scale(combined, moe_out_gain).astype(jnp.bfloat16)
    return (mixer_out, moe_out)


def solution(mesh):
    in_specs = (
        P("ep", "tp"),
        P("tp", None, None),
        P("tp"),
        P("tp", None),
        P(),
        P(("ep", "tp"), None),
        P("ep", None),
        P("ep", None),
        P(),
        P("ep", None, "tp"),
        P("ep", None, "tp"),
        P("ep", "tp", None),
        P(),
    )
    out_specs = (P(("ep", "tp"), None), P(("ep", "tp"), None))
    return jax.shard_map(
        on_device, mesh=mesh, in_specs=in_specs, out_specs=out_specs, check_vma=False
    )
```

profile of v0, /device:TPU:0, one launch (start us, length us, event | category | flops | bytes accessed | tf_op | source)
XLA Modules:
  0.0 171.5 jit_solution(9792254835752840577)
XLA Ops:
  0.6 0.0 copy-start
  0.6 0.0 copy-start.3
  0.7 0.0 copy-start.9
  0.7 0.8 slice.43
  1.5 4.9 %collective-permute-start = (bf16[16,256]{1,0:T(8,128)(2,1)S(1)}, bf16[16,256]{1,0:T(8,128)(2,1)S(1)}, u32[]{:S(2)}, u32[]{:S(2)}) collective-permute-start(bf16[16,256]{1,0:T(8,128)(2,1)S(1)} %slice.43), channel_id=1, source_target_pairs={{0,4},{4,8},{8,12},{12,16},{16,20},{20,24},{24,28},{1,5},{5,9},{9,... | collective-permute-start | bytes 24584 | tf_op jit(solution)/shard_map/ppermute | solution.py:16
  6.4 0.7 constant_dynamic-slice_fusion.1
  7.1 0.1 copy.24
  7.2 0.1 eq.85
  7.4 0.1 eq.81
  7.5 1.2 reduce-window.14
  8.7 0.2 slice_reduce_fusion.2
  8.9 0.1 fusion.30
  9.0 0.1 reduce_sum.39
  9.2 0.1 add_add_fusion
  9.3 0.2 slice_reduce_fusion.1
  9.5 0.0 copy-done.3
  9.5 0.3 fusion.1
  9.8 0.0 copy-start.4
  9.8 0.0 copy-done.9
  9.8 2.5 %convolution_convert_fusion = bf16[640,2048]{1,0:T(8,128)(2,1)} fusion(bf16[256,2048]{1,0:T(8,128)(2,1)S(1)} %copy-done.3, f32[2048]{0:T(1024)S(1)} %copy-done.9, f32[256]{0:T(256)S(1)} %add_rsqrt_fusion.1, s32[256]{0:T(256)S(1)} %get-tuple-element.7, s32[256]{0:T(256)S(1)} %get-tuple-element.6), kind=kOutput, calls=%fused_computation | convolution fusion | flops 674988032 | bytes 3681280 | tf_op jit(solution)/shard_map/dot_general | solution.py:494
  12.3 0.8 constant_dynamic-slice_fusion
  13.2 0.0 collective-permute-done
  13.2 0.0 copy-done.4
  13.2 0.1 fusion.27
  13.3 0.7 fusion.6
  14.0 0.0 copy-start.5
  14.0 0.0 copy-start.8
  14.0 0.1 broadcast_add_fusion
  14.1 0.2 copy.23
  14.4 0.0 copy-done
  14.4 0.5 copy-done.5
  14.9 0.0 copy-done.8
  14.9 2.3 %convolution_convert_fusion.1 = bf16[512,2048]{1,0:T(8,128)(2,1)} fusion(bf16[256,2048]{1,0:T(8,128)(2,1)S(1)} %copy-done, f32[528,256]{1,0:T(8,128)S(1)} %get-tuple-element.9, f32[640,256]{1,0:T(8,128)S(1)} %bitcast.43, f32[528,256]{1,0:T(8,128)S(1)} %slice.57, s32[]{:T(128)S(6)} %select_n.15, f32[256]{0:T(256)S(1)} %copy-done.8, ...), kind=kOutput, calls=%fused_computation.1 | convolution fusion | flops 605814784 | bytes 4852740 | tf_op jit(solution)/shard_map/dot_general | solution.py:499
  17.2 147.8 %shard_map.140 = (bf16[8,80,2048]{2,1,0:T(8,128)(2,1)}, f32[128,2048]{1,0:T(8,128)}) custom-call(bf16[8,80,2048]{2,1,0:T(8,128)(2,1)} %bitcast.49, bf16[4,128,2048]{2,1,0:T(8,128)(2,1)} %bitcast.45, bf16[2,2048,256]{2,1,0:T(8,128)(2,1)} %gate_hbm.1, bf16[2,2048,256]{2,1,0:T(8,128)(2,1)} %up_hbm.1, bf16[2,256,2048]{2,1,0:T(8,128)(2,1)} %down_hbm.1), custom_call_target="tpu_custom_call" | custom-call | flops 16106127360 | bytes 5242880 | tf_op jit(solution)/shard_map/pallas_call | solution.py:396
  165.0 0.0 copy-start.1
  165.0 2.9 %convolution_multiply_fusion = f32[256,2048]{1,0:T(8,128)S(1)} fusion(bf16[640,2048]{1,0:T(8,128)(2,1)} %bitcast.40, f32[256]{0:T(256)S(1)} %bitcast.47, s32[256]{0:T(256)S(1)} %get-tuple-element.7), kind=kOutput, calls=%fused_computation.2 | convolution fusion | flops 671776768 | bytes 4720640 | tf_op jit(solution)/shard_map/dot_general | solution.py:512
  167.9 0.0 copy-done.1
  167.9 0.0 copy-start.2
  167.9 0.0 copy-start.6
  167.9 1.2 multiply_reduce_fusion
  169.2 0.0 copy-start.7
  169.2 0.0 copy-done.2
  169.2 0.2 multiply_reduce_fusion.1
  169.4 0.0 copy-done.6
  169.4 1.0 multiply_convert_fusion.1
  170.3 0.0 copy-done.7
  170.3 1.2 multiply_convert_fusion
  (11 shorter events, 0.2 us)
Async XLA Ops:
  0.6 13.7 %copy-start = (bf16[256,2048]{1,0:T(8,128)(2,1)S(1)}, bf16[256,2048]{1,0:T(8,128)(2,1)}, u32[]{:S(2)}) copy-start(bf16[256,2048]{1,0:T(8,128)(2,1)} %param.16) | copy-start | bytes 3145732
  0.6 8.9 %copy-start.3 = (bf16[256,2048]{1,0:T(8,128)(2,1)S(1)}, bf16[256,2048]{1,0:T(8,128)(2,1)}, u32[]{:S(2)}) copy-start(bf16[256,2048]{1,0:T(8,128)(2,1)} %param.18) | copy-start | bytes 3145732
  0.7 9.2 %copy-start.9 = (f32[2048]{0:T(1024)S(1)}, f32[2048]{0:T(1024)}, u32[]{:S(2)}) copy-start(f32[2048]{0:T(1024)} %param.21) | copy-start | bytes 24580
  1.5 11.7 %collective-permute-start = (bf16[16,256]{1,0:T(8,128)(2,1)S(1)}, bf16[16,256]{1,0:T(8,128)(2,1)S(1)}, u32[]{:S(2)}, u32[]{:S(2)}) collective-permute-start(bf16[16,256]{1,0:T(8,128)(2,1)S(1)} %slice.43), channel_id=1, source_target_pairs={{0,4},{4,8},{8,12},{12,16},{16,20},{20,24},{24,28},{1,5},{5,9},{9,... | collective-permute-start | bytes 24584 | tf_op jit(solution)/shard_map/ppermute | solution.py:16
  9.8 3.4 %copy-start.4 = (bf16[512,256]{1,0:T(8,128)(2,1)S(1)}, bf16[512,256]{1,0:T(8,128)(2,1)}, u32[]{:S(2)}) copy-start(bf16[512,256]{1,0:T(8,128)(2,1)} %param.13) | copy-start | bytes 786436
  14.0 0.9 copy-start.5
  14.0 0.9 copy-start.8
  165.0 2.9 %copy-start.1 = (bf16[8,80,2048]{2,1,0:T(8,128)(2,1)S(1)}, bf16[8,80,2048]{2,1,0:T(8,128)(2,1)}, u32[]{:S(2)}) copy-start(bf16[8,80,2048]{2,1,0:T(8,128)(2,1)} %get-tuple-element.5) | copy-start | bytes 7864324
  167.9 1.3 copy-start.2
  167.9 1.4 copy-start.6
  169.2 1.2 copy-start.7
where the time goes:
time: 172 us
  Pallas kernels  148 us (86%)
  matrix products  8.92 us (5%)
  starting transfers between devices  4.86 us (3%)
  other arithmetic  4.85 us (3%)
  local copies, waits for them, and re-layouts  4.23 us (2%)
    pallas_call x1, Pallas kernels, exchange(): pl.pallas_call(functools.partial(exchange_kernel, capacity), out_shape=(j...  148 us
    ppermute x1, starting transfers between devices, passed_along(): lax.ppermute(value, axis, [(source, source + steps) for source in range(i...  4.86 us
    dot_general x2, matrix products, on_device(): picked = jnp.dot(place, back, preferred_element_type=jnp.float32)  4.16 us
  transfers between devices with their start and end apart: 1, of which 0 were waited for; matrix products, arithmetic and copies ran while one was open for 4% of the time, Pallas kernels for 0%

commit v1 on v0

v1 whole, which is shorter than its diff:
```python
import functools

import jax
import jax.numpy as jnp
from jax import lax
from jax.experimental import pallas as pl
from jax.experimental.pallas import tpu as pltpu
from jax.sharding import PartitionSpec as P

NORM_EPS = 1e-06
MESH = pl.DeviceIdType.MESH
F32 = jnp.float32
BF16 = jnp.bfloat16
ROW_TILE = 16
COMBINE_LAG = 6


def rms_scale(values, gain_vec):
    mean_sq = jnp.mean(values * values, axis=-1, keepdims=True)
    return values * lax.rsqrt(mean_sq + NORM_EPS) * gain_vec


def fused_kernel(
    capacity,
    pool_hbm,
    group_hbm,
    pool_scale,
    out_w_hbm,
    mix_gain,
    tokens_hbm,
    routes,
    route_weights,
    in_gain,
    gate_hbm,
    up_hbm,
    down_hbm,
    out_gain,
    mixer_out,
    moe_out,
    pool,
    history,
    group_w,
    out_w,
    tokens,
    normed,
    slot_rows,
    columns_of,
    outgoing,
    arrived,
    part,
    core_in,
    chip_sum,
    cross_in,
    final,
    returned,
    total_rows,
    gate,
    up,
    down,
    mix_held,
    mix_core,
    mix_sum,
    mix_cross,
    mix_done,
    local_sem,
    hist_sem,
    dis_send,
    dis_recv,
    y1_send,
    y1_recv,
    c1_send,
    c1_recv,
    c2_send,
    c2_recv,
    y2_send,
    y2_recv,
    ret_send,
    ret_recv,
    m1_send,
    m1_recv,
    m2_send,
    m2_recv,
):
    ep_size, tp_size, rows, width = arrived.shape
    exp_dev, _, ff_dev = gate.shape
    tok_dev = tokens.shape[0]
    top_count = routes.shape[0]
    experts = exp_dev * ep_size
    rows_a = pool.shape[0]
    history_rows = history.shape[0]
    highs = tp_size // 2
    ep = lax.axis_index("ep")
    tp = lax.axis_index("tp")
    hi, lo = tp // 2, tp % 2
    other = 1 - lo

    def remote(src, dst, send, recv, to_ep, to_tp):
        return pltpu.make_async_remote_copy(
            src_ref=src,
            dst_ref=dst,
            send_sem=send,
            recv_sem=recv,
            device_id=(to_ep, to_tp),
            device_id_type=MESH,
        )

    def peer_high(k):
        return lax.rem(hi + k, highs)

    def offset_of(i):
        far = jnp.where(i == 0, 1, ep_size - i)
        return jnp.where(i == ep_size - 1, 0, far)

    def partner_ep(d):
        value = ep * 0
        bit = 1
        while bit < ep_size:
            value = value + bit * (((ep // bit) % 2 + (d // bit) % 2) % 2)
            bit *= 2
        return value

    def dispatch(d):
        peer = partner_ep(d)
        return remote(
            outgoing.at[peer], arrived.at[d, tp], dis_send.at[d], dis_recv.at[d], peer, tp
        )

    def gather_cross(d, k):
        slot = arrived.at[d, tp]
        return remote(
            slot, slot, y1_send.at[d, k], y1_recv.at[d, highs - k], ep, peer_high(k) * 2 + lo
        )

    def gather_cross_in(d, k):
        high = peer_high(k)
        slot = arrived.at[d, high * 2 + lo]
        return remote(slot, slot, y1_send.at[d, k], y1_recv.at[d, k], ep, high * 2 + lo)

    def gather_core(d, high):
        slot = arrived.at[d, high * 2 + lo]
        return remote(slot, slot, c1_send.at[d, high], c1_recv.at[d, high], ep, hi * 2 + other)

    def gather_core_in(d, high):
        slot = arrived.at[d, high * 2 + other]
        return remote(slot, slot, c1_send.at[d, high], c1_recv.at[d, high], ep, hi * 2 + other)

    def reduce_core(d, high):
        return remote(
            part.at[high * 2 + other],
            core_in.at[d, high],
            c2_send.at[d, high],
            c2_recv.at[d, high],
            ep,
            hi * 2 + other,
        )

    def reduce_cross(d, k, slot):
        high = peer_high(k)
        return remote(
            chip_sum.at[slot, high],
            cross_in.at[d, highs - k - 1],
            y2_send.at[d, k],
            y2_recv.at[d, highs - k],
            ep,
            high * 2 + lo,
        )

    def reduce_cross_in(d, k, slot):
        high = peer_high(k)
        return remote(
            chip_sum.at[slot, high],
            cross_in.at[d, k - 1],
            y2_send.at[d, k],
            y2_recv.at[d, k],
            ep,
            high * 2 + lo,
        )

    def give_back(d):
        peer = partner_ep(d)
        return remote(final.at[d], returned.at[d], ret_send.at[d], ret_recv.at[d], peer, tp)

    def mix_core_copy(high):
        return remote(
            mix_held.at[high * 2 + other],
            mix_core.at[high],
            m1_send.at[high],
            m1_recv.at[high],
            ep,
            hi * 2 + other,
        )

    def mix_cross_copy(k):
        high = peer_high(k)
        return remote(
            mix_sum.at[high],
            mix_cross.at[highs - k - 1],
            m2_send.at[k],
            m2_recv.at[highs - k],
            ep,
            high * 2 + lo,
        )

    def mix_cross_in(k):
        high = peer_high(k)
        return remote(
            mix_sum.at[high],
            mix_cross.at[k - 1],
            m2_send.at[k],
            m2_recv.at[k],
            ep,
            high * 2 + lo,
        )

    last_rows = pool.at[rows_a - history_rows :]
    send_history = remote(
        last_rows, history, hist_sem.at[0], hist_sem.at[1], jnp.minimum(ep + 1, ep_size - 1), tp
    )

    tokens_copy = pltpu.make_async_copy(tokens_hbm, tokens, local_sem.at[0])
    pool_copy = pltpu.make_async_copy(pool_hbm, pool, local_sem.at[1])
    mixer_copies = [
        pltpu.make_async_copy(group_hbm, group_w, local_sem.at[2]),
        pltpu.make_async_copy(out_w_hbm, out_w, local_sem.at[3]),
    ]
    weight_copies = [
        pltpu.make_async_copy(gate_hbm, gate, local_sem.at[4]),
        pltpu.make_async_copy(up_hbm, up, local_sem.at[5]),
        pltpu.make_async_copy(down_hbm, down, local_sem.at[6]),
    ]
    mixer_store = pltpu.make_async_copy(mix_done, mixer_out, local_sem.at[7])
    moe_store = pltpu.make_async_copy(normed, moe_out, local_sem.at[8])

    tokens_copy.start()
    pool_copy.start()

    barrier = pltpu.get_barrier_semaphore()

    def greet(d, carry):
        pl.semaphore_signal(barrier, inc=1, device_id=(partner_ep(d), tp), device_id_type=MESH)
        return carry

    lax.fori_loop(1, ep_size, greet, 0)
    for k in range(1, highs):
        pl.semaphore_signal(
            barrier, inc=1, device_id=(ep, peer_high(k) * 2 + lo), device_id_type=MESH
        )
    pl.semaphore_signal(barrier, inc=1, device_id=(ep, hi * 2 + other), device_id_type=MESH)
    for copy in mixer_copies + weight_copies:
        copy.start()

    own_tokens = pl.ds(pl.multiple_of(tp * tok_dev, tok_dev), tok_dev)
    own_routes = routes[:, own_tokens]
    own_weights = route_weights[:, own_tokens]
    expert_id = lax.broadcasted_iota(jnp.int32, (experts, tok_dev), 0)
    first_slot = (
        lax.div(expert_id, exp_dev) * rows + lax.rem(expert_id, exp_dev) * capacity
    ).astype(F32)
    earlier = (
        lax.broadcasted_iota(jnp.int32, (tok_dev, tok_dev), 0)
        < lax.broadcasted_iota(jnp.int32, (tok_dev, tok_dev), 1)
    ).astype(BF16)
    taken = jnp.zeros((experts, 1), F32)
    slot_list = []
    for k in range(top_count):
        named = (own_routes[k : k + 1, :] == expert_id).astype(F32)
        before = jnp.dot(named.astype(BF16), earlier, preferred_element_type=F32)
        slot = jnp.sum(named * (before + taken + first_slot), axis=0, keepdims=True)
        taken = taken + jnp.sum(named, axis=1, keepdims=True)
        slot_list.append(slot)
        slot_rows[k : k + 1, :] = slot.astype(jnp.int32)
    stacked = jnp.concatenate(
        slot_list
        + [own_weights[k : k + 1, :] for k in range(top_count)]
        + [jnp.zeros((columns_of.shape[1] - 2 * top_count, tok_dev), F32)],
        axis=0,
    )
    columns_of[...] = stacked.T

    tokens_copy.wait()
    normed[...] = rms_scale(tokens[...].astype(F32), in_gain[...]).astype(BF16)

    def routed_rows(owner):
        slot_id = lax.broadcasted_iota(jnp.int32, (rows, tok_dev), 0) + owner * rows
        chosen = slot_rows[0:1, :] == slot_id
        for k in range(1, top_count):
            chosen = chosen | (slot_rows[k : k + 1, :] == slot_id)
        return jnp.dot(
            chosen.astype(F32).astype(BF16), normed[...], preferred_element_type=F32
        ).astype(BF16)

    pl.semaphore_wait(barrier, ep_size - 1 + highs)

    def stage_a(d):
        for k in range(1, highs):
            gather_cross(d, k).start()
        gather_core(d, hi).start()

    pool_copy.wait()

    @pl.when(ep < ep_size - 1)
    def _():
        send_history.start()

    arrived[0, tp] = routed_rows(ep)
    stage_a(0)

    def send_out(i, carry):
        d = offset_of(i)
        peer = partner_ep(d)
        outgoing[peer] = routed_rows(peer)
        dispatch(d).start()
        return carry

    lax.fori_loop(0, ep_size - 1, send_out, 0)

    for copy in mixer_copies:
        copy.wait()

    @pl.when(ep > 0)
    def _():
        send_history.wait_recv()

    @pl.when(ep == 0)
    def _():
        history[...] = jnp.zeros(history.shape, BF16)

    values = pool[...].astype(F32)
    running = jnp.concatenate([history[...].astype(F32), values], axis=0)
    summed = None
    for group in range(tp_size):
        running = running + pltpu.roll(running, 2**group, 0)
        current = running[history_rows:]
        summed = current if summed is None else jnp.where(tp == group, current, summed)
    window = jnp.int32(1)
    for group in range(tp_size):
        window = jnp.where(tp == group, 2 ** (group + 1), window)
    position = ep * rows_a + lax.broadcasted_iota(jnp.int32, values.shape, 0)
    divisor = jnp.minimum(position + 1, window).astype(F32)
    pooled = (summed / divisor - values).astype(BF16)
    grouped = (
        jnp.dot(pooled, group_w[0], preferred_element_type=F32) * pool_scale[...]
    ).astype(BF16)
    column_step = min(width, 512)
    mix_rows = rows_a // tp_size
    for start in range(0, width, column_step):
        columns = slice(start, start + column_step)
        mix_held[:, :, columns] = (
            jnp.dot(grouped, out_w[:, columns], preferred_element_type=F32)
            .astype(BF16)
            .reshape(tp_size, mix_rows, column_step)
        )
    for high in range(highs):
        mix_core_copy(high).start()
    for high in range(highs):
        mix_core_copy(high).wait_recv()
    for high in range(highs):
        mix_sum[high] = (
            mix_held[high * 2 + lo].astype(F32) + mix_core[high].astype(F32)
        ).astype(BF16)
    for k in range(1, highs):
        mix_cross_copy(k).start()
    first = offset_of(ep * 0)
    dispatch(first).wait_recv()
    stage_a(first)
    for copy in weight_copies:
        copy.wait()
    total_rows[...] = jnp.zeros(total_rows.shape, F32)

    spans = []
    for e in range(exp_dev):
        begin = e * capacity // ROW_TILE * ROW_TILE
        end = -(-(e + 1) * capacity // ROW_TILE) * ROW_TILE
        spans.append((begin, end))
    edges = sorted({0, rows} | {edge for span in spans for edge in span})

    def experts_on(d):
        hidden = []
        for e, (begin, end) in enumerate(spans):
            count = end - begin
            block = arrived[d, :, begin:end, :].reshape(tp_size * count, width)
            gate_act = jnp.dot(block, gate[e], preferred_element_type=F32)
            up_act = jnp.dot(block, up[e], preferred_element_type=F32)
            act = gate_act / (1.0 + jnp.exp(-gate_act)) * up_act
            place = begin + lax.rem(
                lax.broadcasted_iota(jnp.int32, (tp_size * count, 1), 0), count
            )
            mine = (place >= e * capacity) & (place < (e + 1) * capacity)
            hidden.append(jnp.where(mine, act, 0.0).astype(BF16))
        for start in range(0, width, column_step):
            columns = slice(start, start + column_step)
            outs = []
            for e, (begin, end) in enumerate(spans):
                out = jnp.dot(hidden[e], down[e, :, columns], preferred_element_type=F32)
                outs.append(out.reshape(tp_size, end - begin, column_step))
            for begin, end in zip(edges[:-1], edges[1:]):
                piece = None
                for (first_row, last_row), out in zip(spans, outs):
                    if first_row <= begin and end <= last_row:
                        held = out[:, begin - first_row : end - first_row]
                        piece = held if piece is None else piece + held
                if piece is None:
                    piece = jnp.zeros((tp_size, end - begin, column_step), F32)
                part[:, begin:end, columns] = piece.astype(BF16)

    def combine(owner, block):
        slot_id = (
            lax.broadcasted_iota(jnp.int32, (tok_dev, rows), 1) + owner * rows
        ).astype(F32)
        weights = jnp.zeros((tok_dev, rows), F32)
        for k in range(top_count):
            weights = weights + jnp.where(
                columns_of[:, k : k + 1] == slot_id,
                columns_of[:, top_count + k : top_count + k + 1],
                0.0,
            )
        major = weights.astype(BF16)
        minor = (weights - major.astype(F32)).astype(BF16)
        for start in range(0, width, column_step):
            columns = slice(start, start + column_step)
            held = block[:, columns]
            total_rows[:, columns] += jnp.dot(
                major, held, preferred_element_type=F32
            ) + jnp.dot(minor, held, preferred_element_type=F32)

    def combine_from(j):
        d = offset_of(j)
        give_back(d).wait_recv()
        combine(partner_ep(d), returned.at[d])

    def step(i, carry):
        @pl.when(i + 1 < ep_size - 1)
        def _():
            d = offset_of(i + 1)
            dispatch(d).wait_recv()
            stage_a(d)

        @pl.when(i < ep_size)
        def _():
            d = offset_of(i)
            for k in range(1, highs):
                gather_cross_in(d, k).wait_recv()
                gather_core(d, peer_high(k)).start()

        @pl.when(i >= 3)
        def _():
            d = offset_of(i - 3)
            slot = (i - 3) % 2
            total = chip_sum[slot, hi].astype(F32)
            for k in range(1, highs):
                reduce_cross(d, k, slot).wait_send()
                reduce_cross_in(d, k, slot).wait_recv()
                total = total + cross_in[d, k - 1].astype(F32)
            final[d] = total.astype(BF16)

            @pl.when(i < ep_size + 2)
            def _():
                give_back(d).start()

        @pl.when((i >= 1) & (i <= ep_size))
        def _():
            d = offset_of(i - 1)
            slot = (i - 1) % 2
            for high in range(highs):
                reduce_core(d, high).wait_recv()
                reduce_core(d, high).wait_send()
                chip_sum[slot, high] = (
                    part[high * 2 + lo].astype(F32) + core_in[d, high].astype(F32)
                ).astype(BF16)
            for k in range(1, highs):
                reduce_cross(d, k, slot).start()

        @pl.when(i < ep_size)
        def _():
            d = offset_of(i)
            for high in range(highs):
                gather_core_in(d, high).wait_recv()
            experts_on(d)
            for high in range(highs):
                reduce_core(d, high).start()

        @pl.when(i == 2)
        def _():
            total = mix_sum[hi].astype(F32)
            for k in range(1, highs):
                mix_cross_in(k).wait_recv()
                total = total + mix_cross[k - 1].astype(F32)
            mix_done[...] = rms_scale(total, mix_gain[...]).astype(BF16)
            mixer_store.start()

        @pl.when(i >= COMBINE_LAG)
        def _():
            combine_from(i - COMBINE_LAG)

        return carry

    lax.fori_loop(0, ep_size + 3, step, 0)

    def late(j, carry):
        combine_from(j)
        return carry

    lax.fori_loop(max(0, ep_size + 3 - COMBINE_LAG), ep_size - 1, late, 0)
    combine(ep, final.at[0])
    normed[...] = rms_scale(total_rows[...], out_gain[...]).astype(BF16)
    moe_store.start()

    for k in range(1, highs):
        mix_cross_copy(k).wait_send()
    for high in range(highs):
        mix_core_copy(high).wait_send()

    @pl.when(ep < ep_size - 1)
    def _():
        send_history.wait_send()

    def drain_all(d, carry):
        for k in range(1, highs):
            gather_cross(d, k).wait_send()
        for high in range(highs):
            gather_core(d, high).wait_send()
        return carry

    lax.fori_loop(0, ep_size, drain_all, 0)

    def drain(d, carry):
        dispatch(d).wait_send()
        give_back(d).wait_send()
        return carry

    lax.fori_loop(1, ep_size, drain, 0)
    mixer_store.wait()
    moe_store.wait()


def on_device(
    pool_input,
    group_weight,
    pool_scale,
    out_weight,
    mix_gain,
    expert_input,
    routes,
    route_weights,
    moe_in_gain,
    gate_weight,
    up_weight,
    down_weight,
    moe_out_gain,
):
    tp_size = lax.axis_size("tp")
    ep_size = lax.axis_size("ep")
    rows_a, group_width = pool_input.shape
    width = out_weight.shape[1]
    exp_dev = gate_weight.shape[0]
    experts = exp_dev * ep_size
    tok_dev = expert_input.shape[0]
    top_count = routes.shape[1]
    capacity = max(2, 5 * tok_dev * top_count // (4 * experts))
    rows = -(-exp_dev * capacity // ROW_TILE) * ROW_TILE
    highs = tp_size // 2
    mix_rows = rows_a // tp_size
    history_rows = 2**tp_size
    any_spec = pl.BlockSpec(memory_space=pl.ANY)
    vmem_spec = pl.BlockSpec(memory_space=pltpu.VMEM)
    dma = pltpu.SemaphoreType.DMA
    pair = (ep_size, highs)
    flops = 6 * gate_weight.size * ep_size * tp_size * rows
    mixer_out, moe_out = pl.pallas_call(
        functools.partial(fused_kernel, capacity),
        out_shape=(
            jax.ShapeDtypeStruct((mix_rows, width), BF16),
            jax.ShapeDtypeStruct((tok_dev, width), BF16),
        ),
        in_specs=[
            any_spec,
            any_spec,
            vmem_spec,
            any_spec,
            vmem_spec,
            any_spec,
            vmem_spec,
            vmem_spec,
            vmem_spec,
            any_spec,
            any_spec,
            any_spec,
            vmem_spec,
        ],
        out_specs=(any_spec, any_spec),
        scratch_shapes=[
            pltpu.VMEM(pool_input.shape, BF16),
            pltpu.VMEM((history_rows, group_width), BF16),
            pltpu.VMEM(group_weight.shape, BF16),
            pltpu.VMEM(out_weight.shape, BF16),
            pltpu.VMEM(expert_input.shape, BF16),
            pltpu.VMEM(expert_input.shape, BF16),
            pltpu.VMEM((8, tok_dev), jnp.int32),
            pltpu.VMEM((tok_dev, 8), F32),
            pltpu.VMEM((ep_size, rows, width), BF16),
            pltpu.VMEM((ep_size, tp_size, rows, width), BF16),
            pltpu.VMEM((tp_size, rows, width), BF16),
            pltpu.VMEM((ep_size, highs, rows, width), BF16),
            pltpu.VMEM((2, highs, rows, width), BF16),
            pltpu.VMEM((ep_size, highs - 1, rows, width), BF16),
            pltpu.VMEM((ep_size, rows, width), BF16),
            pltpu.VMEM((ep_size, rows, width), BF16),
            pltpu.VMEM(expert_input.shape, F32),
            pltpu.VMEM(gate_weight.shape, BF16),
            pltpu.VMEM(up_weight.shape, BF16),
            pltpu.VMEM(down_weight.shape, BF16),
            pltpu.VMEM((tp_size, mix_rows, width), BF16),
            pltpu.VMEM((highs, mix_rows, width), BF16),
            pltpu.VMEM((highs, mix_rows, width), BF16),
            pltpu.VMEM((highs - 1, mix_rows, width), BF16),
            pltpu.VMEM((mix_rows, width), BF16),
            dma((9,)),
            dma((2,)),
            dma((ep_size,)),
            dma((ep_size,)),
            dma(pair),
            dma(pair),
            dma(pair),
            dma(pair),
            dma(pair),
            dma(pair),
            dma(pair),
            dma(pair),
            dma((ep_size,)),
            dma((ep_size,)),
            dma((highs,)),
            dma((highs,)),
            dma((highs,)),
            dma((highs,)),
        ],
        compiler_params=pltpu.CompilerParams(
            collective_id=0, has_side_effects=True, vmem_limit_bytes=60 * 1024 * 1024
        ),
        cost_estimate=pl.CostEstimate(
            flops=flops, bytes_accessed=8 * expert_input.size, transcendentals=0
        ),
    )(
        pool_input,
        group_weight,
        pool_scale.reshape(1, -1),
        out_weight,
        mix_gain.reshape(1, -1),
        expert_input,
        routes.T,
        route_weights.T,
        moe_in_gain.reshape(1, -1),
        gate_weight,
        up_weight,
        down_weight,
        moe_out_gain.reshape(1, -1),
    )
    return (mixer_out, moe_out)


def solution(mesh):
    in_specs = (
        P("ep", "tp"),
        P("tp", None, None),
        P("tp"),
        P("tp", None),
        P(),
        P(("ep", "tp"), None),
        P("ep", None),
        P("ep", None),
        P(),
        P("ep", None, "tp"),
        P("ep", None, "tp"),
        P("ep", "tp", None),
        P(),
    )
    out_specs = (P(("ep", "tp"), None), P(("ep", "tp"), None))
    return jax.shard_map(
        on_device, mesh=mesh, in_specs=in_specs, out_specs=out_specs, check_vma=False
    )
```

time: 172 us -> 167 us (0.971)
  Pallas kernels: 148 us -> 162 us
  matrix products: 8.92 us -> 0 us
  starting transfers between devices: 4.86 us -> 0 us
  other arithmetic: 4.85 us -> 0 us
    pallas_call x1, Pallas kernels: 148 us -> 162 us  [on_device(): pl.pallas_call(functools.partial(fused_kernel, capacity), out_shape=(jax....]
    dot_general x4 -> x0, matrix products: 8.92 us -> none  [the longest x2 4.16 us: on_device(): picked = jnp.dot(place, back, preferred_element_type=jnp.float32)]
    ppermute x1 -> x0, starting transfers between devices: 4.86 us -> none  [passed_along(): lax.ppermute(value, axis, [(source, source + steps) for source in range(i...]
    unnamed x21 -> x2, local copies, waits for them, and re-layouts: 0.71 us -> 4.18 us
    convert_element_type x4 -> x0, other arithmetic: 2.17 us -> none  [the longest x1 1.21 us: on_device(): moe_out = rms_scale(combined, moe_out_gain).astype(jnp.bfloat16)]
    slice x4 -> x0, local copies, waits for them, and re-layouts: 2.09 us -> none  [the longest x1 0.85 us: on_device(): history = passed_along(pool_input[rows_a - history_rows:], 'ep', 1)]
    another operation x6 -> x0, other arithmetic: 2.01 us -> none
  transfers between devices with their start and end apart: 1 -> 0, of which waited for: 0 -> 0; matrix products, arithmetic and copies ran while one was open for 4% -> 0% of each run, Pallas kernels for 0% -> 0%
where the time goes in v1:
time: 167 us
  Pallas kernels  162 us (97%)
  local copies, waits for them, and re-layouts  4.18 us (3%)
    pallas_call x1, Pallas kernels, on_device(): pl.pallas_call(functools.partial(fused_kernel, capacity), out_shape=(jax....  162 us
    unnamed x2, local copies, waits for them, and re-layouts  4.18 us

profile of v1, /device:TPU:0, one launch (start us, length us, event | category | flops | bytes accessed | tf_op | source)
XLA Modules:
  0.0 166.6 jit_solution(9402797616633990982)
XLA Ops:
  0.6 161.8 %shard_map.140 = (bf16[128,2048]{1,0:T(8,128)(2,1)}, bf16[256,2048]{1,0:T(8,128)(2,1)}) custom-call(bf16[512,256]{1,0:T(8,128)(2,1)} %pool_hbm.1, bf16[1,256,256]{2,1,0:T(8,128)(2,1)} %group_hbm.1, f32[1,256]{1,0:T(1,128)} %bitcast.11, bf16[256,2048]{1,0:T(8,128)(2,1)} %out_w_hbm.1, f32[1,2048]{1,0:T(1,128)} %bitcast.6, bf16[256,2048]{1,0:T(8,128)(2,1)} %tokens_hbm.1, ...), custom_call_target="tpu_custom_call" | custom-call | flops 16106127360 | bytes 4194304 | tf_op jit(solution)/shard_map/pallas_call | solution.py:569
  162.4 1.9 %copy.17 = bf16[128,2048]{1,0:T(8,128)(2,1)} copy(bf16[128,2048]{1,0:T(8,128)(2,1)} %get-tuple-element.4) | data formatting | bytes 1048576
  164.3 2.3 %copy.18 = bf16[256,2048]{1,0:T(8,128)(2,1)} copy(bf16[256,2048]{1,0:T(8,128)(2,1)} %get-tuple-element.5) | data formatting | bytes 2097152

commit v2 on v1

--- a/solution.py
+++ b/solution.py
@@ -1,4 +1,5 @@
 import functools
+import math
 
 import jax
 import jax.numpy as jnp
@@ -8,12 +9,51 @@
 from jax.sharding import PartitionSpec as P
 
 NORM_EPS = 1e-06
+ROOM = 56 * 1024 * 1024
+SPARE = 3 * 1024 * 1024
 MESH = pl.DeviceIdType.MESH
 F32 = jnp.float32
 BF16 = jnp.bfloat16
 ROW_TILE = 16
-COMBINE_LAG = 6
-
+GATHER, FORWARD, COMPUTE, REDUCE, RETURN, COMBINE, MIX, NONE = range(8)
+KINDS = {
+    "A": GATHER,
+    "X": FORWARD,
+    "C": COMPUTE,
+    "R": REDUCE,
+    "F": RETURN,
+    "B": COMBINE,
+    "M": MIX,
+}
+STEADY = (
+    (GATHER, -1, 1),
+    (FORWARD, 0, 0),
+    (RETURN, 3, 0),
+    (REDUCE, 1, 0),
+    (COMPUTE, 0, 0),
+    (COMBINE, 8, 1),
+)
+CODE_BITS = 6
+PER_WORD = 5
+
+
+def coded(*events):
+    return tuple(KINDS[event[0]] * 8 + int(event[1:] or 0) for event in events)
+
+
+END_EVENTS = coded(
+    "A3", "A1", "A6", "A7", "X6", "C6", "R6", "A4", "X7", "C7", "R7", "A5", "F6", "X4", "C4",
+    "R4", "F7", "X5", "C5", "R5", "F4", "X1", "C1", "R1", "A2", "F5", "X3", "C3", "R3", "F1",
+    "X2", "C2", "R2", "F3", "X0", "C0", "R0", "M", "F2", "B6", "B7", "B4", "B5", "B1", "B3",
+    "F0", "B2",
+)
+MIDDLE_EVENTS = coded(
+    "A1", "A4", "A5", "X4", "C4", "R4", "X5", "C5", "R5", "F4", "X1", "C1", "R1", "F5", "A3",
+    "A6", "X3", "C3", "R3", "F1", "X6", "C6", "R6", "A7", "A2", "F3", "F6", "X7", "C7", "R7",
+    "X2", "C2", "R2", "F7", "X0", "C0", "R0", "M", "F2", "B4", "B5", "B1", "B3", "B6", "B7",
+    "F0", "B2",
+)
+SEND_ORDER = (1, 4, 5, 6, 7, 3, 2)
 
 def rms_scale(values, gain_vec):
     mean_sq = jnp.mean(values * values, axis=-1, keepdims=True)
@@ -24,19 +64,25 @@
     capacity,
     pool_hbm,
     group_hbm,
+    pool_scale_hbm,
+    out_w_hbm,
+    mix_gain_hbm,
+    tokens_hbm,
+    routes_hbm,
+    route_weights_hbm,
+    in_gain_hbm,
+    gate_hbm,
+    up_hbm,
+    down_hbm,
+    out_gain_hbm,
+    mixer_out,
+    moe_out,
     pool_scale,
-    out_w_hbm,
     mix_gain,
-    tokens_hbm,
     routes,
     route_weights,
     in_gain,
-    gate_hbm,
-    up_hbm,
-    down_hbm,
     out_gain,
-    mixer_out,
-    moe_out,
     pool,
     history,
     group_w,
@@ -49,9 +95,7 @@
     arrived,
     part,
     core_in,
-    chip_sum,
     cross_in,
-    final,
     returned,
     total_rows,
     gate,
@@ -61,7 +105,6 @@
     mix_core,
     mix_sum,
     mix_cross,
-    mix_done,
     local_sem,
     hist_sem,
     dis_send,
@@ -107,9 +150,42 @@
     def peer_high(k):
         return lax.rem(hi + k, highs)
 
+    on_end = (ep // 2) % 2 == (ep // 4) % 2
+    tabled = ep_size == 8
+
+    def packed_at(table, i):
+        words = []
+        for begin in range(0, len(table), PER_WORD):
+            piece = table[begin : begin + PER_WORD]
+            words.append(sum(value << (CODE_BITS * at) for at, value in enumerate(piece)))
+        word = jnp.int32(words[0])
+        for at in range(1, len(words)):
+            word = jnp.where(i >= at * PER_WORD, words[at], word)
+        shift = CODE_BITS * lax.rem(i, PER_WORD)
+        return lax.rem(lax.shift_right_logical(word, shift), 1 << CODE_BITS)
+
     def offset_of(i):
         far = jnp.where(i == 0, 1, ep_size - i)
         return jnp.where(i == ep_size - 1, 0, far)
+
+    def sent_at(i):
+        if tabled:
+            return packed_at(SEND_ORDER, i)
+        return offset_of(i)
+
+    def event_at(t):
+        if tabled:
+            code = jnp.where(on_end, packed_at(END_EVENTS, t), packed_at(MIDDLE_EVENTS, t))
+            return code // 8, code % 8
+        i, slot = t // 8, t % 8
+        op, j = jnp.int32(NONE), i
+        for at, (kind, lag, last) in enumerate(STEADY):
+            index = i - lag
+            valid = (slot == at) & (index >= 0) & (index < ep_size - last)
+            op = jnp.where(valid, kind, op)
+            j = jnp.where(valid, index, j)
+        op = jnp.where((slot == 6) & (i == 0), MIX, op)
+        return op, offset_of(j)
 
     def partner_ep(d):
         value = ep * 0
@@ -154,10 +230,10 @@
             hi * 2 + other,
         )
 
-    def reduce_cross(d, k, slot):
+    def reduce_cross(d, k):
         high = peer_high(k)
         return remote(
-            chip_sum.at[slot, high],
+            core_in.at[d, high],
             cross_in.at[d, highs - k - 1],
             y2_send.at[d, k],
             y2_recv.at[d, highs - k],
@@ -165,10 +241,10 @@
             high * 2 + lo,
         )
 
-    def reduce_cross_in(d, k, slot):
+    def reduce_cross_in(d, k):
         high = peer_high(k)
         return remote(
-            chip_sum.at[slot, high],
+            core_in.at[d, high],
             cross_in.at[d, k - 1],
             y2_send.at[d, k],
             y2_recv.at[d, k],
@@ -178,7 +254,7 @@
 
     def give_back(d):
         peer = partner_ep(d)
-        return remote(final.at[d], returned.at[d], ret_send.at[d], ret_recv.at[d], peer, tp)
+        return remote(core_in.at[d, hi], returned.at[d], ret_send.at[d], ret_recv.at[d], peer, tp)
 
     def mix_core_copy(high):
         return remote(
@@ -228,9 +304,19 @@
         pltpu.make_async_copy(up_hbm, up, local_sem.at[5]),
         pltpu.make_async_copy(down_hbm, down, local_sem.at[6]),
     ]
-    mixer_store = pltpu.make_async_copy(mix_done, mixer_out, local_sem.at[7])
-    moe_store = pltpu.make_async_copy(normed, moe_out, local_sem.at[8])
-
+
+    early_copies = [
+        pltpu.make_async_copy(routes_hbm, routes, local_sem.at[9]),
+        pltpu.make_async_copy(route_weights_hbm, route_weights, local_sem.at[10]),
+        pltpu.make_async_copy(in_gain_hbm, in_gain, local_sem.at[11]),
+    ]
+    mixer_copies += [
+        pltpu.make_async_copy(pool_scale_hbm, pool_scale, local_sem.at[12]),
+        pltpu.make_async_copy(mix_gain_hbm, mix_gain, local_sem.at[13]),
+        pltpu.make_async_copy(out_gain_hbm, out_gain, local_sem.at[14]),
+    ]
+    for copy in early_copies:
+        copy.start()
     tokens_copy.start()
     pool_copy.start()
 
@@ -250,6 +336,8 @@
         copy.start()
 
     own_tokens = pl.ds(pl.multiple_of(tp * tok_dev, tok_dev), tok_dev)
+    for copy in early_copies:
+        copy.wait()
     own_routes = routes[:, own_tokens]
     own_weights = route_weights[:, own_tokens]
     expert_id = lax.broadcasted_iota(jnp.int32, (experts, tok_dev), 0)
@@ -289,24 +377,72 @@
             chosen.astype(F32).astype(BF16), normed[...], preferred_element_type=F32
         ).astype(BF16)
 
-    pl.semaphore_wait(barrier, ep_size - 1 + highs)
+    column_step = min(width, 512)
+
+    def mixer_part():
+        for copy in mixer_copies:
+            copy.wait()
+
+        @pl.when(ep > 0)
+        def _():
+            send_history.wait_recv()
+
+        @pl.when(ep == 0)
+        def _():
+            history[...] = jnp.zeros(history.shape, BF16)
+
+        values = pool[...].astype(F32)
+        running = jnp.concatenate([history[...].astype(F32), values], axis=0)
+        summed = None
+        for group in range(tp_size):
+            running = running + pltpu.roll(running, 2**group, 0)
+            current = running[history_rows:]
+            summed = current if summed is None else jnp.where(tp == group, current, summed)
+        window = jnp.int32(1)
+        for group in range(tp_size):
+            window = jnp.where(tp == group, 2 ** (group + 1), window)
+        position = ep * rows_a + lax.broadcasted_iota(jnp.int32, values.shape, 0)
+        divisor = jnp.minimum(position + 1, window).astype(F32)
+        pooled = (summed / divisor - values).astype(BF16)
+        grouped = (
+            jnp.dot(pooled, group_w[0], preferred_element_type=F32) * pool_scale[...]
+        ).astype(BF16)
+        mix_rows = rows_a // tp_size
+        for start in range(0, width, column_step):
+            columns = slice(start, start + column_step)
+            mix_held[:, :, columns] = (
+                jnp.dot(grouped, out_w[:, columns], preferred_element_type=F32)
+                .astype(BF16)
+                .reshape(tp_size, mix_rows, column_step)
+            )
+        for high in range(highs):
+            mix_core_copy(high).start()
+        for high in range(highs):
+            mix_core_copy(high).wait_recv()
+        for high in range(highs):
+            mix_sum[high] = (
+                mix_held[high * 2 + lo].astype(F32) + mix_core[high].astype(F32)
+            ).astype(BF16)
+        for k in range(1, highs):
+            mix_cross_copy(k).start()
 
     def stage_a(d):
         for k in range(1, highs):
             gather_cross(d, k).start()
         gather_core(d, hi).start()
 
+    arrived[0, tp] = routed_rows(ep)
     pool_copy.wait()
+    pl.semaphore_wait(barrier, ep_size - 1 + highs)
 
     @pl.when(ep < ep_size - 1)
     def _():
         send_history.start()
 
-    arrived[0, tp] = routed_rows(ep)
     stage_a(0)
 
     def send_out(i, carry):
-        d = offset_of(i)
+        d = sent_at(i)
         peer = partner_ep(d)
         outgoing[peer] = routed_rows(peer)
         dispatch(d).start()
@@ -314,55 +450,12 @@
 
     lax.fori_loop(0, ep_size - 1, send_out, 0)
 
-    for copy in mixer_copies:
-        copy.wait()
-
-    @pl.when(ep > 0)
-    def _():
-        send_history.wait_recv()
-
-    @pl.when(ep == 0)
-    def _():
-        history[...] = jnp.zeros(history.shape, BF16)
-
-    values = pool[...].astype(F32)
-    running = jnp.concatenate([history[...].astype(F32), values], axis=0)
-    summed = None
-    for group in range(tp_size):
-        running = running + pltpu.roll(running, 2**group, 0)
-        current = running[history_rows:]
-        summed = current if summed is None else jnp.where(tp == group, current, summed)
-    window = jnp.int32(1)
-    for group in range(tp_size):
-        window = jnp.where(tp == group, 2 ** (group + 1), window)
-    position = ep * rows_a + lax.broadcasted_iota(jnp.int32, values.shape, 0)
-    divisor = jnp.minimum(position + 1, window).astype(F32)
-    pooled = (summed / divisor - values).astype(BF16)
-    grouped = (
-        jnp.dot(pooled, group_w[0], preferred_element_type=F32) * pool_scale[...]
-    ).astype(BF16)
-    column_step = min(width, 512)
-    mix_rows = rows_a // tp_size
-    for start in range(0, width, column_step):
-        columns = slice(start, start + column_step)
-        mix_held[:, :, columns] = (
-            jnp.dot(grouped, out_w[:, columns], preferred_element_type=F32)
-            .astype(BF16)
-            .reshape(tp_size, mix_rows, column_step)
-        )
-    for high in range(highs):
-        mix_core_copy(high).start()
-    for high in range(highs):
-        mix_core_copy(high).wait_recv()
-    for high in range(highs):
-        mix_sum[high] = (
-            mix_held[high * 2 + lo].astype(F32) + mix_core[high].astype(F32)
-        ).astype(BF16)
-    for k in range(1, highs):
-        mix_cross_copy(k).start()
-    first = offset_of(ep * 0)
-    dispatch(first).wait_recv()
-    stage_a(first)
+    def gather_next(d):
+        dispatch(d).wait_recv()
+        stage_a(d)
+
+    if not tabled:
+        gather_next(offset_of(ep * 0))
     for copy in weight_copies:
         copy.wait()
     total_rows[...] = jnp.zeros(total_rows.shape, F32)
@@ -404,106 +497,96 @@
                 part[:, begin:end, columns] = piece.astype(BF16)
 
     def combine(owner, block):
-        slot_id = (
-            lax.broadcasted_iota(jnp.int32, (tok_dev, rows), 1) + owner * rows
-        ).astype(F32)
-        weights = jnp.zeros((tok_dev, rows), F32)
+        lane = lax.broadcasted_iota(jnp.int32, (tok_dev, 2 * rows), 1)
+        slot_id = (lax.rem(lane, rows) + owner * rows).astype(F32)
+        weights = jnp.zeros((tok_dev, 2 * rows), F32)
         for k in range(top_count):
             weights = weights + jnp.where(
                 columns_of[:, k : k + 1] == slot_id,
                 columns_of[:, top_count + k : top_count + k + 1],
                 0.0,
             )
-        major = weights.astype(BF16)
-        minor = (weights - major.astype(F32)).astype(BF16)
+        major = weights.astype(BF16).astype(F32)
+        split = jnp.where(lane < rows, major, weights - major).astype(BF16)
         for start in range(0, width, column_step):
             columns = slice(start, start + column_step)
             held = block[:, columns]
-            total_rows[:, columns] += jnp.dot(
-                major, held, preferred_element_type=F32
-            ) + jnp.dot(minor, held, preferred_element_type=F32)
-
-    def combine_from(j):
-        d = offset_of(j)
+            twice = jnp.concatenate([held, held], axis=0)
+            total_rows[:, columns] += jnp.dot(split, twice, preferred_element_type=F32)
+
+    def combine_from(d):
         give_back(d).wait_recv()
         combine(partner_ep(d), returned.at[d])
 
-    def step(i, carry):
-        @pl.when(i + 1 < ep_size - 1)
+    def forward(d):
+        for k in range(1, highs):
+            gather_cross_in(d, k).wait_recv()
+            gather_core(d, peer_high(k)).start()
+
+    def compute(d):
+        for high in range(highs):
+            gather_core_in(d, high).wait_recv()
+        experts_on(d)
+        for high in range(highs):
+            reduce_core(d, high).start()
+
+    def reduce(d):
+        for high in range(highs):
+            reduce_core(d, high).wait_recv()
+            reduce_core(d, high).wait_send()
+            core_in[d, high] = (
+                part[high * 2 + lo].astype(F32) + core_in[d, high].astype(F32)
+            ).astype(BF16)
+        for k in range(1, highs):
+            reduce_cross(d, k).start()
+
+    def send_home(d):
+        total = core_in[d, hi].astype(F32)
+        for k in range(1, highs):
+            reduce_cross_in(d, k).wait_recv()
+            total = total + cross_in[d, k - 1].astype(F32)
+        core_in[d, hi] = total.astype(BF16)
+
+        @pl.when(d != 0)
         def _():
-            d = offset_of(i + 1)
-            dispatch(d).wait_recv()
-            stage_a(d)
-
-        @pl.when(i < ep_size)
-        def _():
-            d = offset_of(i)
-            for k in range(1, highs):
-                gather_cross_in(d, k).wait_recv()
-                gather_core(d, peer_high(k)).start()
-
-        @pl.when(i >= 3)
-        def _():
-            d = offset_of(i - 3)
-            slot = (i - 3) % 2
-            total = chip_sum[slot, hi].astype(F32)
-            for k in range(1, highs):
-                reduce_cross(d, k, slot).wait_send()
-                reduce_cross_in(d, k, slot).wait_recv()
-                total = total + cross_in[d, k - 1].astype(F32)
-            final[d] = total.astype(BF16)
-
-            @pl.when(i < ep_size + 2)
-            def _():
-                give_back(d).start()
-
-        @pl.when((i >= 1) & (i <= ep_size))
-        def _():
-            d = offset_of(i - 1)
-            slot = (i - 1) % 2
-            for high in range(highs):
-                reduce_core(d, high).wait_recv()
-                reduce_core(d, high).wait_send()
-                chip_sum[slot, high] = (
-                    part[high * 2 + lo].astype(F32) + core_in[d, high].astype(F32)
-                ).astype(BF16)
-            for k in range(1, highs):
-                reduce_cross(d, k, slot).start()
-
-        @pl.when(i < ep_size)
-        def _():
-            d = offset_of(i)
-            for high in range(highs):
-                gather_core_in(d, high).wait_recv()
-            experts_on(d)
-            for high in range(highs):
-                reduce_core(d, high).start()
-
-        @pl.when(i == 2)
-        def _():
-            total = mix_sum[hi].astype(F32)
-            for k in range(1, highs):
-                mix_cross_in(k).wait_recv()
-                total = total + mix_cross[k - 1].astype(F32)
-            mix_done[...] = rms_scale(total, mix_gain[...]).astype(BF16)
-            mixer_store.start()
-
-        @pl.when(i >= COMBINE_LAG)
-        def _():
-            combine_from(i - COMBINE_LAG)
-
+            give_back(d).start()
+
+    def mixer_end():
+        total = mix_sum[hi].astype(F32)
+        for k in range(1, highs):
+            mix_cross_in(k).wait_recv()
+            total = total + mix_cross[k - 1].astype(F32)
+        mixer_out[...] = rms_scale(total, mix_gain[...]).astype(BF16)
+
+    actions = {
+        GATHER: gather_next,
+        FORWARD: forward,
+        COMPUTE: compute,
+        REDUCE: reduce,
+        RETURN: send_home,
+        COMBINE: combine_from,
+        MIX: lambda d: mixer_part(),
+    }
+
+    def event(t, carry):
+        op, d = event_at(t)
+        for kind, action in actions.items():
+            pl.when(op == kind)(functools.partial(action, d))
         return carry
 
-    lax.fori_loop(0, ep_size + 3, step, 0)
-
-    def late(j, carry):
-        combine_from(j)
-        return carry
-
-    lax.fori_loop(max(0, ep_size + 3 - COMBINE_LAG), ep_size - 1, late, 0)
-    combine(ep, final.at[0])
-    normed[...] = rms_scale(total_rows[...], out_gain[...]).astype(BF16)
-    moe_store.start()
+    count = len(END_EVENTS) if tabled else 8 * (ep_size + 3)
+    lax.fori_loop(0, count, event, 0)
+
+    if not tabled:
+
+        def late(j, carry):
+            combine_from(offset_of(j))
+            return carry
+
+        lax.fori_loop(max(0, ep_size - 5), ep_size - 1, late, 0)
+    combine(ep, core_in.at[0, hi])
+    moe_out[...] = rms_scale(total_rows[...], out_gain[...]).astype(BF16)
+    mixer_end()
 
     for k in range(1, highs):
         mix_cross_copy(k).wait_send()
@@ -517,6 +600,7 @@
     def drain_all(d, carry):
         for k in range(1, highs):
             gather_cross(d, k).wait_send()
+            reduce_cross(d, k).wait_send()
         for high in range(highs):
             gather_core(d, high).wait_send()
         return carry
@@ -529,8 +613,6 @@
         return carry
 
     lax.fori_loop(1, ep_size, drain, 0)
-    mixer_store.wait()
-    moe_store.wait()
 
 
 def on_device(
@@ -561,80 +643,75 @@
     highs = tp_size // 2
     mix_rows = rows_a // tp_size
     history_rows = 2**tp_size
-    any_spec = pl.BlockSpec(memory_space=pl.ANY)
     vmem_spec = pl.BlockSpec(memory_space=pltpu.VMEM)
+    hbm_spec = pl.BlockSpec(memory_space=pltpu.HBM)
     dma = pltpu.SemaphoreType.DMA
     pair = (ep_size, highs)
     flops = 6 * gate_weight.size * ep_size * tp_size * rows
+    scratch = [
+        pltpu.VMEM((1, group_width), F32),
+        pltpu.VMEM((1, width), F32),
+        pltpu.VMEM((top_count, tok_dev * tp_size), jnp.int32),
+        pltpu.VMEM((top_count, tok_dev * tp_size), F32),
+        pltpu.VMEM((1, width), F32),
+        pltpu.VMEM((1, width), F32),
+        pltpu.VMEM(pool_input.shape, BF16),
+        pltpu.VMEM((history_rows, group_width), BF16),
+        pltpu.VMEM(group_weight.shape, BF16),
+        pltpu.VMEM(out_weight.shape, BF16),
+        pltpu.VMEM(expert_input.shape, BF16),
+        pltpu.VMEM(expert_input.shape, BF16),
+        pltpu.VMEM((8, tok_dev), jnp.int32),
+        pltpu.VMEM((tok_dev, 8), F32),
+        pltpu.VMEM((ep_size, rows, width), BF16),
+        pltpu.VMEM((ep_size, tp_size, rows, width), BF16),
+        pltpu.VMEM((tp_size, rows, width), BF16),
+        pltpu.VMEM((ep_size, highs, rows, width), BF16),
+        pltpu.VMEM((ep_size, highs - 1, rows, width), BF16),
+        pltpu.VMEM((ep_size, rows, width), BF16),
+        pltpu.VMEM(expert_input.shape, F32),
+        pltpu.VMEM(gate_weight.shape, BF16),
+        pltpu.VMEM(up_weight.shape, BF16),
+        pltpu.VMEM(down_weight.shape, BF16),
+        pltpu.VMEM((tp_size, mix_rows, width), BF16),
+        pltpu.VMEM((highs, mix_rows, width), BF16),
+        pltpu.VMEM((highs, mix_rows, width), BF16),
+        pltpu.VMEM((highs - 1, mix_rows, width), BF16),
+        dma((15,)),
+        dma((2,)),
+        dma((ep_size,)),
+        dma((ep_size,)),
+        dma(pair),
+        dma(pair),
+        dma(pair),
+        dma(pair),
+        dma(pair),
+        dma(pair),
+        dma(pair),
+        dma(pair),
+        dma((ep_size,)),
+        dma((ep_size,)),
+        dma((highs,)),
+        dma((highs,)),
+        dma((highs,)),
+        dma((highs,)),
+    ]
+    held = sum(
+        ref.dtype.itemsize * math.prod(ref.shape)
+        for ref in scratch
+        if ref.memory_space == pltpu.VMEM
+    )
     mixer_out, moe_out = pl.pallas_call(
         functools.partial(fused_kernel, capacity),
         out_shape=(
-            jax.ShapeDtypeStruct((mix_rows, width), BF16),
-            jax.ShapeDtypeStruct((tok_dev, width), BF16),
+            pltpu.VMEM((mix_rows, width), BF16),
+            pltpu.VMEM((tok_dev, width), BF16),
         ),
-        in_specs=[
-            any_spec,
-            any_spec,
-            vmem_spec,
-            any_spec,
-            vmem_spec,
-            any_spec,
-            vmem_spec,
-            vmem_spec,
-            vmem_spec,
-            any_spec,
-            any_spec,
-            any_spec,
-            vmem_spec,
-        ],
-        out_specs=(any_spec, any_spec),
-        scratch_shapes=[
-            pltpu.VMEM(pool_input.shape, BF16),
-            pltpu.VMEM((history_rows, group_width), BF16),
-            pltpu.VMEM(group_weight.shape, BF16),
-            pltpu.VMEM(out_weight.shape, BF16),
-            pltpu.VMEM(expert_input.shape, BF16),
-            pltpu.VMEM(expert_input.shape, BF16),
-            pltpu.VMEM((8, tok_dev), jnp.int32),
-            pltpu.VMEM((tok_dev, 8), F32),
-            pltpu.VMEM((ep_size, rows, width), BF16),
-            pltpu.VMEM((ep_size, tp_size, rows, width), BF16),
-            pltpu.VMEM((tp_size, rows, width), BF16),
-            pltpu.VMEM((ep_size, highs, rows, width), BF16),
-            pltpu.VMEM((2, highs, rows, width), BF16),
-            pltpu.VMEM((ep_size, highs - 1, rows, width), BF16),
-            pltpu.VMEM((ep_size, rows, width), BF16),
-            pltpu.VMEM((ep_size, rows, width), BF16),
-            pltpu.VMEM(expert_input.shape, F32),
-            pltpu.VMEM(gate_weight.shape, BF16),
-            pltpu.VMEM(up_weight.shape, BF16),
-            pltpu.VMEM(down_weight.shape, BF16),
-            pltpu.VMEM((tp_size, mix_rows, width), BF16),
-            pltpu.VMEM((highs, mix_rows, width), BF16),
-            pltpu.VMEM((highs, mix_rows, width), BF16),
-            pltpu.VMEM((highs - 1, mix_rows, width), BF16),
-            pltpu.VMEM((mix_rows, width), BF16),
-            dma((9,)),
-            dma((2,)),
-            dma((ep_size,)),
-            dma((ep_size,)),
-            dma(pair),
-            dma(pair),
-            dma(pair),
-            dma(pair),
-            dma(pair),
-            dma(pair),
-            dma(pair),
-            dma(pair),
-            dma((ep_size,)),
-            dma((ep_size,)),
-            dma((highs,)),
-            dma((highs,)),
-            dma((highs,)),
-            dma((highs,)),
-        ],
+        in_specs=[hbm_spec] * 13,
+        out_specs=(vmem_spec, vmem_spec),
+        scratch_shapes=scratch,
         compiler_params=pltpu.CompilerParams(
-            collective_id=0, has_side_effects=True, vmem_limit_bytes=60 * 1024 * 1024
+            collective_id=0, has_side_effects=True, vmem_limit_bytes=max(ROOM, held + SPARE)
         ),
         cost_estimate=pl.CostEstimate(
             flops=flops, bytes_accessed=8 * expert_input.size, transcendentals=0

time: 167 us -> 140 us (0.84)
  Pallas kernels: 162 us -> 137 us
  local copies, waits for them, and re-layouts: 4.18 us -> 1.77 us
    pallas_call x1, Pallas kernels: 162 us -> 137 us  [on_device(): pl.pallas_call(functools.partial(fused_kernel, capacity), out_shape=(pltp...]
    unnamed x2, local copies, waits for them, and re-layouts: 4.18 us -> 1.77 us
where the time goes in v2:
time: 140 us; the launch traced here: 139 us
  Pallas kernels  137 us (98%)
  local copies, waits for them, and re-layouts  1.77 us (1%)
    pallas_call x1, Pallas kernels, on_device(): pl.pallas_call(functools.partial(fused_kernel, capacity), out_shape=(pltp...  137 us

profile of v2, /device:TPU:0, one launch (start us, length us, event | category | flops | bytes accessed | tf_op | source)
XLA Modules:
  0.0 139.4 jit_solution(13857149993167539892)
XLA Ops:
  0.6 137.0 %shard_map.140 = (bf16[128,2048]{1,0:T(8,128)(2,1)S(1)}, bf16[256,2048]{1,0:T(8,128)(2,1)S(1)}) custom-call(bf16[512,256]{1,0:T(8,128)(2,1)} %pool_hbm.1, bf16[1,256,256]{2,1,0:T(8,128)(2,1)} %group_hbm.1, f32[1,256]{1,0:T(1,128)} %bitcast.11, bf16[256,2048]{1,0:T(8,128)(2,1)} %out_w_hbm.1, f32[1,2048]{1,0:T(1,128)} %bitcast.6, ...), custom_call_target="tpu_custom_call" | custom-call | flops 16106127360 | bytes 4194304 | tf_op jit(solution)/shard_map/pallas_call | solution.py:704
  137.6 0.8 copy.17
  138.4 1.0 copy.18

commit v3 on v2

--- a/solution.py
+++ b/solution.py
@@ -15,7 +15,7 @@
 F32 = jnp.float32
 BF16 = jnp.bfloat16
 ROW_TILE = 16
-GATHER, FORWARD, COMPUTE, REDUCE, RETURN, COMBINE, MIX, NONE = range(8)
+GATHER, FORWARD, COMPUTE, REDUCE, RETURN, COMBINE, MIX, PEER, NONE = range(9)
 KINDS = {
     "A": GATHER,
     "X": FORWARD,
@@ -24,6 +24,7 @@
     "F": RETURN,
     "B": COMBINE,
     "M": MIX,
+    "P": PEER,
 }
 STEADY = (
     (GATHER, -1, 1),
@@ -34,6 +35,7 @@
     (COMBINE, 8, 1),
 )
 CODE_BITS = 6
+NEAR = 4
 PER_WORD = 5
 
 
@@ -42,16 +44,16 @@
 
 
 END_EVENTS = coded(
-    "A3", "A1", "A6", "A7", "X6", "C6", "R6", "A4", "X7", "C7", "R7", "A5", "F6", "X4", "C4",
-    "R4", "F7", "X5", "C5", "R5", "F4", "X1", "C1", "R1", "A2", "F5", "X3", "C3", "R3", "F1",
-    "X2", "C2", "R2", "F3", "X0", "C0", "R0", "M", "F2", "B6", "B7", "B4", "B5", "B1", "B3",
-    "F0", "B2",
+    "A3", "A1", "A6", "P", "A7", "X6", "C6", "R6", "X7", "C7", "R7", "A4", "A5", "F6", "F7",
+    "X4", "C4", "R4", "X5", "C5", "R5", "F4", "A2", "X1", "C1", "R1", "F5", "X3", "C3", "R3",
+    "F1", "X2", "C2", "R2", "F3", "X0", "C0", "R0", "M", "F2", "B6", "B7", "B4", "B5", "B1",
+    "B3", "F0", "B2",
 )
 MIDDLE_EVENTS = coded(
-    "A1", "A4", "A5", "X4", "C4", "R4", "X5", "C5", "R5", "F4", "X1", "C1", "R1", "F5", "A3",
-    "A6", "X3", "C3", "R3", "F1", "X6", "C6", "R6", "A7", "A2", "F3", "F6", "X7", "C7", "R7",
-    "X2", "C2", "R2", "F7", "X0", "C0", "R0", "M", "F2", "B4", "B5", "B1", "B3", "B6", "B7",
-    "F0", "B2",
+    "A1", "A4", "A5", "P", "X4", "C4", "R4", "X5", "C5", "R5", "F4", "X0", "C0", "R0", "F5",
+    "A6", "X1", "C1", "R1", "F0", "X6", "C6", "R6", "A7", "A3", "F1", "X3", "C3", "R3", "F6",
+    "A2", "X7", "C7", "R7", "F3", "X2", "C2", "R2", "F7", "M", "B4", "B5", "F2", "B1", "B3",
+    "B6", "B7", "B2",
 )
 SEND_ORDER = (1, 4, 5, 6, 7, 3, 2)
 
@@ -89,6 +91,8 @@
     out_w,
     tokens,
     normed,
+    raw,
+    near_out,
     slot_rows,
     columns_of,
     outgoing,
@@ -107,6 +111,8 @@
     mix_cross,
     local_sem,
     hist_sem,
+    raw_send,
+    raw_recv,
     dis_send,
     dis_recv,
     y1_send,
@@ -252,6 +258,31 @@
             high * 2 + lo,
         )
 
+    def raw_copy(k):
+        return remote(
+            normed,
+            raw.at[highs - k - 1],
+            raw_send.at[k],
+            raw_recv.at[highs - k],
+            ep,
+            peer_high(k) * 2 + lo,
+        )
+
+    def raw_copy_in(k):
+        return remote(
+            normed, raw.at[k - 1], raw_send.at[k], raw_recv.at[k], ep, peer_high(k) * 2 + lo
+        )
+
+    def near_copy(d, k):
+        return remote(
+            near_out.at[d, k - 1],
+            arrived.at[d, peer_high(k) * 2 + lo],
+            y1_send.at[d, k],
+            y1_recv.at[d, k],
+            partner_ep(d),
+            tp,
+        )
+
     def give_back(d):
         peer = partner_ep(d)
         return remote(core_in.at[d, hi], returned.at[d], ret_send.at[d], ret_recv.at[d], peer, tp)
@@ -335,11 +366,6 @@
     for copy in mixer_copies + weight_copies:
         copy.start()
 
-    own_tokens = pl.ds(pl.multiple_of(tp * tok_dev, tok_dev), tok_dev)
-    for copy in early_copies:
-        copy.wait()
-    own_routes = routes[:, own_tokens]
-    own_weights = route_weights[:, own_tokens]
     expert_id = lax.broadcasted_iota(jnp.int32, (experts, tok_dev), 0)
     first_slot = (
         lax.div(expert_id, exp_dev) * rows + lax.rem(expert_id, exp_dev) * capacity
@@ -348,15 +374,39 @@
         lax.broadcasted_iota(jnp.int32, (tok_dev, tok_dev), 0)
         < lax.broadcasted_iota(jnp.int32, (tok_dev, tok_dev), 1)
     ).astype(BF16)
-    taken = jnp.zeros((experts, 1), F32)
-    slot_list = []
-    for k in range(top_count):
-        named = (own_routes[k : k + 1, :] == expert_id).astype(F32)
-        before = jnp.dot(named.astype(BF16), earlier, preferred_element_type=F32)
-        slot = jnp.sum(named * (before + taken + first_slot), axis=0, keepdims=True)
-        taken = taken + jnp.sum(named, axis=1, keepdims=True)
-        slot_list.append(slot)
-        slot_rows[k : k + 1, :] = slot.astype(jnp.int32)
+
+    def tokens_of(index):
+        return pl.ds(pl.multiple_of(index * tok_dev, tok_dev), tok_dev)
+
+    def find_slots(index, base):
+        block_routes = routes[:, tokens_of(index)]
+        taken = jnp.zeros((experts, 1), F32)
+        found = []
+        for k in range(top_count):
+            named = (block_routes[k : k + 1, :] == expert_id).astype(F32)
+            before = jnp.dot(named.astype(BF16), earlier, preferred_element_type=F32)
+            slot = jnp.sum(named * (before + taken + first_slot), axis=0, keepdims=True)
+            taken = taken + jnp.sum(named, axis=1, keepdims=True)
+            found.append(slot)
+            slot_rows[base + k : base + k + 1, :] = slot.astype(jnp.int32)
+        return found
+
+    for copy in early_copies:
+        copy.wait()
+    tokens_copy.wait()
+    normed[...] = rms_scale(tokens[...].astype(F32), in_gain[...]).astype(BF16)
+    pool_copy.wait()
+    pl.semaphore_wait(barrier, ep_size - 1 + highs)
+    if tabled:
+        for k in range(1, highs):
+            raw_copy(k).start()
+
+    @pl.when(ep < ep_size - 1)
+    def _():
+        send_history.start()
+
+    slot_list = find_slots(tp, 0)
+    own_weights = route_weights[:, tokens_of(tp)]
     stacked = jnp.concatenate(
         slot_list
         + [own_weights[k : k + 1, :] for k in range(top_count)]
@@ -365,16 +415,13 @@
     )
     columns_of[...] = stacked.T
 
-    tokens_copy.wait()
-    normed[...] = rms_scale(tokens[...].astype(F32), in_gain[...]).astype(BF16)
-
-    def routed_rows(owner):
+    def routed_rows(owner, base, source):
         slot_id = lax.broadcasted_iota(jnp.int32, (rows, tok_dev), 0) + owner * rows
-        chosen = slot_rows[0:1, :] == slot_id
+        chosen = slot_rows[base : base + 1, :] == slot_id
         for k in range(1, top_count):
-            chosen = chosen | (slot_rows[k : k + 1, :] == slot_id)
+            chosen = chosen | (slot_rows[base + k : base + k + 1, :] == slot_id)
         return jnp.dot(
-            chosen.astype(F32).astype(BF16), normed[...], preferred_element_type=F32
+            chosen.astype(F32).astype(BF16), source[...], preferred_element_type=F32
         ).astype(BF16)
 
     column_step = min(width, 512)
@@ -427,24 +474,38 @@
             mix_cross_copy(k).start()
 
     def stage_a(d):
+        def cross():
+            for k in range(1, highs):
+                gather_cross(d, k).start()
+
+        if tabled:
+            pl.when(d >= NEAR)(cross)
+        else:
+            cross()
+        gather_core(d, hi).start()
+
+    def peer_blocks():
         for k in range(1, highs):
-            gather_cross(d, k).start()
-        gather_core(d, hi).start()
-
-    arrived[0, tp] = routed_rows(ep)
-    pool_copy.wait()
-    pl.semaphore_wait(barrier, ep_size - 1 + highs)
-
-    @pl.when(ep < ep_size - 1)
-    def _():
-        send_history.start()
-
-    stage_a(0)
+            base = k * top_count
+            source = raw.at[k - 1]
+            find_slots(peer_high(k) * 2 + lo, base)
+            raw_copy_in(k).wait_recv()
+
+            def send_near(d, carry):
+                near_out[d, k - 1] = routed_rows(partner_ep(d), base, source)
+                near_copy(d, k).start()
+                return carry
+
+            lax.fori_loop(1, NEAR, send_near, 0)
+            arrived[0, peer_high(k) * 2 + lo] = routed_rows(ep, base, source)
+
+    arrived[0, tp] = routed_rows(ep, 0, normed)
+    stage_a(jnp.int32(0))
 
     def send_out(i, carry):
         d = sent_at(i)
         peer = partner_ep(d)
-        outgoing[peer] = routed_rows(peer)
+        outgoing[peer] = routed_rows(peer, 0, normed)
         dispatch(d).start()
         return carry
 
@@ -520,7 +581,14 @@
 
     def forward(d):
         for k in range(1, highs):
-            gather_cross_in(d, k).wait_recv()
+
+            def arrival():
+                gather_cross_in(d, k).wait_recv()
+
+            if tabled:
+                pl.when(d != 0)(arrival)
+            else:
+                arrival()
             gather_core(d, peer_high(k)).start()
 
     def compute(d):
@@ -566,7 +634,11 @@
         RETURN: send_home,
         COMBINE: combine_from,
         MIX: lambda d: mixer_part(),
+        PEER: lambda d: peer_blocks(),
     }
+
+    if not tabled:
+        del actions[PEER]
 
     def event(t, carry):
         op, d = event_at(t)
@@ -586,10 +658,7 @@
         lax.fori_loop(max(0, ep_size - 5), ep_size - 1, late, 0)
     combine(ep, core_in.at[0, hi])
     moe_out[...] = rms_scale(total_rows[...], out_gain[...]).astype(BF16)
-    mixer_end()
-
-    for k in range(1, highs):
-        mix_cross_copy(k).wait_send()
+
     for high in range(highs):
         mix_core_copy(high).wait_send()
 
@@ -597,9 +666,20 @@
     def _():
         send_history.wait_send()
 
+    if tabled:
+        for k in range(1, highs):
+            raw_copy(k).wait_send()
+
     def drain_all(d, carry):
         for k in range(1, highs):
-            gather_cross(d, k).wait_send()
+
+            def gathered():
+                gather_cross(d, k).wait_send()
+
+            if tabled:
+                pl.when(d != 0)(gathered)
+            else:
+                gathered()
             reduce_cross(d, k).wait_send()
         for high in range(highs):
             gather_core(d, high).wait_send()
@@ -613,6 +693,9 @@
         return carry
 
     lax.fori_loop(1, ep_size, drain, 0)
+    mixer_end()
+    for k in range(1, highs):
+        mix_cross_copy(k).wait_send()
 
 
 def on_device(
@@ -643,6 +726,9 @@
     highs = tp_size // 2
     mix_rows = rows_a // tp_size
     history_rows = 2**tp_size
+    tabled = ep_size == 8
+    raw_rows = tok_dev if tabled else ROW_TILE
+    near_rows = rows if tabled else ROW_TILE
     vmem_spec = pl.BlockSpec(memory_space=pltpu.VMEM)
     hbm_spec = pl.BlockSpec(memory_space=pltpu.HBM)
     dma = pltpu.SemaphoreType.DMA
@@ -661,6 +747,8 @@
         pltpu.VMEM(out_weight.shape, BF16),
         pltpu.VMEM(expert_input.shape, BF16),
         pltpu.VMEM(expert_input.shape, BF16),
+        pltpu.VMEM((highs - 1, raw_rows, width), BF16),
+        pltpu.VMEM((NEAR, highs - 1, near_rows, width), BF16),
         pltpu.VMEM((8, tok_dev), jnp.int32),
         pltpu.VMEM((tok_dev, 8), F32),
         pltpu.VMEM((ep_size, rows, width), BF16),
@@ -679,6 +767,8 @@
         pltpu.VMEM((highs - 1, mix_rows, width), BF16),
         dma((15,)),
         dma((2,)),
+        dma((highs,)),
+        dma((highs,)),
         dma((ep_size,)),
         dma((ep_size,)),
         dma(pair),

time: 140 us -> 134 us (0.957)
  Pallas kernels: 137 us -> 131 us
    pallas_call x1, Pallas kernels: 137 us -> 131 us  [on_device(): pl.pallas_call(functools.partial(fused_kernel, capacity), out_shape=(pltp...]
where the time goes in v3:
time: 134 us
  Pallas kernels  131 us (98%)
  local copies, waits for them, and re-layouts  1.77 us (1%)
    pallas_call x1, Pallas kernels, on_device(): pl.pallas_call(functools.partial(fused_kernel, capacity), out_shape=(pltp...  131 us

profile of v3, /device:TPU:0, one launch (start us, length us, event | category | flops | bytes accessed | tf_op | source)
XLA Modules:
  0.0 133.6 jit_solution(2753033639760246284)
XLA Ops:
  0.6 131.2 %shard_map.140 = (bf16[128,2048]{1,0:T(8,128)(2,1)S(1)}, bf16[256,2048]{1,0:T(8,128)(2,1)S(1)}) custom-call(bf16[512,256]{1,0:T(8,128)(2,1)} %pool_hbm.1, bf16[1,256,256]{2,1,0:T(8,128)(2,1)} %group_hbm.1, f32[1,256]{1,0:T(1,128)} %bitcast.11, bf16[256,2048]{1,0:T(8,128)(2,1)} %out_w_hbm.1, f32[1,2048]{1,0:T(1,128)} %bitcast.6, ...), custom_call_target="tpu_custom_call" | custom-call | flops 16106127360 | bytes 4194304 | tf_op jit(solution)/shard_map/pallas_call | solution.py:794
  131.8 0.8 copy.17
  132.6 1.0 copy.18

commit v4 on v3

--- a/solution.py
+++ b/solution.py
@@ -44,18 +44,19 @@
 
 
 END_EVENTS = coded(
-    "A3", "A1", "A6", "P", "A7", "X6", "C6", "R6", "X7", "C7", "R7", "A4", "A5", "F6", "F7",
+    "A6", "A7", "A1", "P", "A3", "X6", "C6", "R6", "X7", "C7", "R7", "F6", "A4", "F7", "A5",
     "X4", "C4", "R4", "X5", "C5", "R5", "F4", "A2", "X1", "C1", "R1", "F5", "X3", "C3", "R3",
     "F1", "X2", "C2", "R2", "F3", "X0", "C0", "R0", "M", "F2", "B6", "B7", "B4", "B5", "B1",
     "B3", "F0", "B2",
 )
 MIDDLE_EVENTS = coded(
-    "A1", "A4", "A5", "P", "X4", "C4", "R4", "X5", "C5", "R5", "F4", "X0", "C0", "R0", "F5",
+    "A1", "A4", "P", "A5", "X4", "C4", "R4", "X5", "C5", "R5", "F4", "X0", "C0", "R0", "F5",
     "A6", "X1", "C1", "R1", "F0", "X6", "C6", "R6", "A7", "A3", "F1", "X3", "C3", "R3", "F6",
     "A2", "X7", "C7", "R7", "F3", "X2", "C2", "R2", "F7", "M", "B4", "B5", "F2", "B1", "B3",
     "B6", "B7", "B2",
 )
-SEND_ORDER = (1, 4, 5, 6, 7, 3, 2)
+END_SENDS = (1, 6, 7, 4, 5, 3, 2)
+MIDDLE_SENDS = (1, 4, 5, 6, 7, 3, 2)
 
 def rms_scale(values, gain_vec):
     mean_sq = jnp.mean(values * values, axis=-1, keepdims=True)
@@ -109,6 +110,7 @@
     mix_core,
     mix_sum,
     mix_cross,
+    mix_done,
     local_sem,
     hist_sem,
     raw_send,
@@ -176,7 +178,7 @@
 
     def sent_at(i):
         if tabled:
-            return packed_at(SEND_ORDER, i)
+            return jnp.where(on_end, packed_at(END_SENDS, i), packed_at(MIDDLE_SENDS, i))
         return offset_of(i)
 
     def event_at(t):
@@ -204,45 +206,55 @@
     def dispatch(d):
         peer = partner_ep(d)
         return remote(
-            outgoing.at[peer], arrived.at[d, tp], dis_send.at[d], dis_recv.at[d], peer, tp
+            outgoing.at[peer], arrived.at[d, tp], dis_send.at[0], dis_recv.at[d], peer, tp
         )
 
     def gather_cross(d, k):
         slot = arrived.at[d, tp]
         return remote(
-            slot, slot, y1_send.at[d, k], y1_recv.at[d, highs - k], ep, peer_high(k) * 2 + lo
+            slot, slot, y1_send.at[k - 1], y1_recv.at[d, highs - k - 1], ep, peer_high(k) * 2 + lo
         )
 
     def gather_cross_in(d, k):
         high = peer_high(k)
         slot = arrived.at[d, high * 2 + lo]
-        return remote(slot, slot, y1_send.at[d, k], y1_recv.at[d, k], ep, high * 2 + lo)
+        return remote(slot, slot, y1_send.at[k - 1], y1_recv.at[d, k - 1], ep, high * 2 + lo)
 
     def gather_core(d, high):
         slot = arrived.at[d, high * 2 + lo]
-        return remote(slot, slot, c1_send.at[d, high], c1_recv.at[d, high], ep, hi * 2 + other)
-
-    def gather_core_in(d, high):
-        slot = arrived.at[d, high * 2 + other]
-        return remote(slot, slot, c1_send.at[d, high], c1_recv.at[d, high], ep, hi * 2 + other)
+        return remote(slot, slot, c1_send.at[0], c1_recv.at[d], ep, hi * 2 + other)
+
+    def gather_core_in(d):
+        slots = arrived.at[d, 0:highs]
+        return remote(slots, slots, c1_send.at[0], c1_recv.at[d], ep, hi * 2 + other)
 
     def reduce_core(d, high):
         return remote(
             part.at[high * 2 + other],
             core_in.at[d, high],
-            c2_send.at[d, high],
-            c2_recv.at[d, high],
+            c2_send.at[0],
+            c2_recv.at[d],
             ep,
             hi * 2 + other,
         )
 
+    def reduce_core_all(d):
+        return remote(
+            part.at[0:highs],
+            core_in.at[d],
+            c2_send.at[0],
+            c2_recv.at[d],
+            ep,
+            hi * 2 + other,
+        )
+
     def reduce_cross(d, k):
         high = peer_high(k)
         return remote(
             core_in.at[d, high],
             cross_in.at[d, highs - k - 1],
-            y2_send.at[d, k],
-            y2_recv.at[d, highs - k],
+            y2_send.at[k - 1],
+            y2_recv.at[d, highs - k - 1],
             ep,
             high * 2 + lo,
         )
@@ -252,8 +264,8 @@
         return remote(
             core_in.at[d, high],
             cross_in.at[d, k - 1],
-            y2_send.at[d, k],
-            y2_recv.at[d, k],
+            y2_send.at[k - 1],
+            y2_recv.at[d, k - 1],
             ep,
             high * 2 + lo,
         )
@@ -262,48 +274,53 @@
         return remote(
             normed,
             raw.at[highs - k - 1],
-            raw_send.at[k],
-            raw_recv.at[highs - k],
+            raw_send.at[k - 1],
+            raw_recv.at[highs - k - 1],
             ep,
             peer_high(k) * 2 + lo,
         )
 
     def raw_copy_in(k):
         return remote(
-            normed, raw.at[k - 1], raw_send.at[k], raw_recv.at[k], ep, peer_high(k) * 2 + lo
+            normed, raw.at[k - 1], raw_send.at[k - 1], raw_recv.at[k - 1], ep, peer_high(k) * 2 + lo
         )
 
     def near_copy(d, k):
         return remote(
             near_out.at[d, k - 1],
             arrived.at[d, peer_high(k) * 2 + lo],
-            y1_send.at[d, k],
-            y1_recv.at[d, k],
+            y1_send.at[k - 1],
+            y1_recv.at[d, k - 1],
             partner_ep(d),
             tp,
         )
 
     def give_back(d):
         peer = partner_ep(d)
-        return remote(core_in.at[d, hi], returned.at[d], ret_send.at[d], ret_recv.at[d], peer, tp)
+        return remote(core_in.at[d, hi], returned.at[d], ret_send.at[0], ret_recv.at[d], peer, tp)
 
     def mix_core_copy(high):
         return remote(
             mix_held.at[high * 2 + other],
             mix_core.at[high],
-            m1_send.at[high],
-            m1_recv.at[high],
+            m1_send.at[0],
+            m1_recv.at[0],
             ep,
             hi * 2 + other,
         )
 
+    def mix_core_all():
+        return remote(
+            mix_held.at[0:highs], mix_core, m1_send.at[0], m1_recv.at[0], ep, hi * 2 + other
+        )
+
     def mix_cross_copy(k):
         high = peer_high(k)
         return remote(
             mix_sum.at[high],
             mix_cross.at[highs - k - 1],
-            m2_send.at[k],
-            m2_recv.at[highs - k],
+            m2_send.at[k - 1],
+            m2_recv.at[highs - k - 1],
             ep,
             high * 2 + lo,
         )
@@ -313,8 +330,8 @@
         return remote(
             mix_sum.at[high],
             mix_cross.at[k - 1],
-            m2_send.at[k],
-            m2_recv.at[k],
+            m2_send.at[k - 1],
+            m2_recv.at[k - 1],
             ep,
             high * 2 + lo,
         )
@@ -324,6 +341,16 @@
         last_rows, history, hist_sem.at[0], hist_sem.at[1], jnp.minimum(ep + 1, ep_size - 1), tp
     )
 
+    half_rows = mix_done.shape[0] // 2
+    mixer_stores = [
+        pltpu.make_async_copy(
+            mix_done.at[half * half_rows : (half + 1) * half_rows],
+            mixer_out.at[half * half_rows : (half + 1) * half_rows],
+            local_sem.at[7 + half],
+        )
+        for half in range(2)
+    ]
+    moe_store = pltpu.make_async_copy(normed, moe_out, local_sem.at[15])
     tokens_copy = pltpu.make_async_copy(tokens_hbm, tokens, local_sem.at[0])
     pool_copy = pltpu.make_async_copy(pool_hbm, pool, local_sem.at[1])
     mixer_copies = [
@@ -464,8 +491,7 @@
             )
         for high in range(highs):
             mix_core_copy(high).start()
-        for high in range(highs):
-            mix_core_copy(high).wait_recv()
+        mix_core_all().wait_recv()
         for high in range(highs):
             mix_sum[high] = (
                 mix_held[high * 2 + lo].astype(F32) + mix_core[high].astype(F32)
@@ -592,16 +618,15 @@
             gather_core(d, peer_high(k)).start()
 
     def compute(d):
-        for high in range(highs):
-            gather_core_in(d, high).wait_recv()
+        gather_core_in(d).wait_recv()
         experts_on(d)
         for high in range(highs):
             reduce_core(d, high).start()
 
     def reduce(d):
+        reduce_core_all(d).wait_recv()
+        reduce_core_all(d).wait_send()
         for high in range(highs):
-            reduce_core(d, high).wait_recv()
-            reduce_core(d, high).wait_send()
             core_in[d, high] = (
                 part[high * 2 + lo].astype(F32) + core_in[d, high].astype(F32)
             ).astype(BF16)
@@ -620,11 +645,15 @@
             give_back(d).start()
 
     def mixer_end():
-        total = mix_sum[hi].astype(F32)
         for k in range(1, highs):
             mix_cross_in(k).wait_recv()
-            total = total + mix_cross[k - 1].astype(F32)
-        mixer_out[...] = rms_scale(total, mix_gain[...]).astype(BF16)
+        for half, store in enumerate(mixer_stores):
+            span = slice(half * half_rows, (half + 1) * half_rows)
+            total = mix_sum[hi, span, :].astype(F32)
+            for k in range(1, highs):
+                total = total + mix_cross[k - 1, span, :].astype(F32)
+            mix_done[span, :] = rms_scale(total, mix_gain[...]).astype(BF16)
+            store.start()
 
     actions = {
         GATHER: gather_next,
@@ -657,45 +686,34 @@
 
         lax.fori_loop(max(0, ep_size - 5), ep_size - 1, late, 0)
     combine(ep, core_in.at[0, hi])
-    moe_out[...] = rms_scale(total_rows[...], out_gain[...]).astype(BF16)
-
-    for high in range(highs):
-        mix_core_copy(high).wait_send()
+    if tabled:
+        for k in range(1, highs):
+            raw_copy(k).wait_send()
+    normed[...] = rms_scale(total_rows[...], out_gain[...]).astype(BF16)
+    moe_store.start()
+
+    mix_core_all().wait_send()
 
     @pl.when(ep < ep_size - 1)
     def _():
         send_history.wait_send()
 
-    if tabled:
-        for k in range(1, highs):
-            raw_copy(k).wait_send()
-
-    def drain_all(d, carry):
-        for k in range(1, highs):
-
-            def gathered():
-                gather_cross(d, k).wait_send()
-
-            if tabled:
-                pl.when(d != 0)(gathered)
-            else:
-                gathered()
-            reduce_cross(d, k).wait_send()
-        for high in range(highs):
-            gather_core(d, high).wait_send()
-        return carry
-
-    lax.fori_loop(0, ep_size, drain_all, 0)
-
-    def drain(d, carry):
-        dispatch(d).wait_send()
-        give_back(d).wait_send()
-        return carry
-
-    lax.fori_loop(1, ep_size, drain, 0)
+    def drain(blocks, sem):
+        remote(blocks, blocks, sem, dis_recv.at[0], ep, hi * 2 + other).wait_send()
+
+    others = outgoing.at[0 : ep_size - 1]
+    for k in range(1, highs):
+        drain(others if tabled else outgoing, y1_send.at[k - 1])
+        drain(outgoing, y2_send.at[k - 1])
+    drain(core_in, c1_send.at[0])
+    drain(others, dis_send.at[0])
+    drain(others, ret_send.at[0])
     mixer_end()
     for k in range(1, highs):
         mix_cross_copy(k).wait_send()
+    moe_store.wait()
+    for store in mixer_stores:
+        store.wait()
 
 
 def on_device(
@@ -729,10 +747,9 @@
     tabled = ep_size == 8
     raw_rows = tok_dev if tabled else ROW_TILE
     near_rows = rows if tabled else ROW_TILE
-    vmem_spec = pl.BlockSpec(memory_space=pltpu.VMEM)
+    any_spec = pl.BlockSpec(memory_space=pl.ANY)
     hbm_spec = pl.BlockSpec(memory_space=pltpu.HBM)
     dma = pltpu.SemaphoreType.DMA
-    pair = (ep_size, highs)
     flops = 6 * gate_weight.size * ep_size * tp_size * rows
     scratch = [
         pltpu.VMEM((1, group_width), F32),
@@ -765,26 +782,27 @@
         pltpu.VMEM((highs, mix_rows, width), BF16),
         pltpu.VMEM((highs, mix_rows, width), BF16),
         pltpu.VMEM((highs - 1, mix_rows, width), BF16),
-        dma((15,)),
+        pltpu.VMEM((mix_rows, width), BF16),
+        dma((16,)),
         dma((2,)),
-        dma((highs,)),
-        dma((highs,)),
+        dma((highs - 1,)),
+        dma((highs - 1,)),
+        dma((1,)),
         dma((ep_size,)),
+        dma((highs - 1,)),
+        dma((ep_size, highs - 1)),
+        dma((1,)),
         dma((ep_size,)),
-        dma(pair),
-        dma(pair),
-        dma(pair),
-        dma(pair),
-        dma(pair),
-        dma(pair),
-        dma(pair),
-        dma(pair),
+        dma((1,)),
         dma((ep_size,)),
+        dma((highs - 1,)),
+        dma((ep_size, highs - 1)),
+        dma((1,)),
         dma((ep_size,)),
-        dma((highs,)),
-        dma((highs,)),
-        dma((highs,)),
-        dma((highs,)),
+        dma((1,)),
+        dma((1,)),
+        dma((highs - 1,)),
+        dma((highs - 1,)),
     ]
     held = sum(
         ref.dtype.itemsize * math.prod(ref.shape)
@@ -798,7 +816,7 @@
             pltpu.VMEM((tok_dev, width), BF16),
         ),
         in_specs=[hbm_spec] * 13,
-        out_specs=(vmem_spec, vmem_spec),
+        out_specs=(any_spec, any_spec),
         scratch_shapes=scratch,
         compiler_params=pltpu.CompilerParams(
             collective_id=0, has_side_effects=True, vmem_limit_bytes=max(ROOM, held + SPARE)

time: 134 us -> 133 us (level)
  no operation moved by 1% of the time
where the time goes in v4:
time: 133 us
  Pallas kernels  130 us (98%)
  local copies, waits for them, and re-layouts  1.77 us (1%)
    pallas_call x1, Pallas kernels, on_device(): pl.pallas_call(functools.partial(fused_kernel, capacity), out_shape=(pltp...  130 us

profile of v4, /device:TPU:0, one launch (start us, length us, event | category | flops | bytes accessed | tf_op | source)
XLA Modules:
  0.0 132.8 jit_solution(10777393333919390247)
XLA Ops:
  0.6 130.4 %shard_map.140 = (bf16[128,2048]{1,0:T(8,128)(2,1)S(1)}, bf16[256,2048]{1,0:T(8,128)(2,1)S(1)}) custom-call(bf16[512,256]{1,0:T(8,128)(2,1)} %pool_hbm.1, bf16[1,256,256]{2,1,0:T(8,128)(2,1)} %group_hbm.1, f32[1,256]{1,0:T(1,128)} %bitcast.11, bf16[256,2048]{1,0:T(8,128)(2,1)} %out_w_hbm.1, f32[1,2048]{1,0:T(1,128)} %bitcast.6, ...), custom_call_target="tpu_custom_call" | custom-call | flops 16106127360 | bytes 4194304 | tf_op jit(solution)/shard_map/pallas_call | solution.py:812
  131.0 0.8 copy.17
  131.8 1.0 copy.18

commit v5 on v4

--- a/solution.py
+++ b/solution.py
@@ -44,7 +44,7 @@
 
 
 END_EVENTS = coded(
-    "A6", "A7", "A1", "P", "A3", "X6", "C6", "R6", "X7", "C7", "R7", "F6", "A4", "F7", "A5",
+    "A6", "A1", "P", "A7", "A3", "X6", "C6", "R6", "X7", "C7", "R7", "F6", "A4", "F7", "A5",
     "X4", "C4", "R4", "X5", "C5", "R5", "F4", "A2", "X1", "C1", "R1", "F5", "X3", "C3", "R3",
     "F1", "X2", "C2", "R2", "F3", "X0", "C0", "R0", "M", "F2", "B6", "B7", "B4", "B5", "B1",
     "B3", "F0", "B2",
@@ -373,11 +373,8 @@
         pltpu.make_async_copy(mix_gain_hbm, mix_gain, local_sem.at[13]),
         pltpu.make_async_copy(out_gain_hbm, out_gain, local_sem.at[14]),
     ]
-    for copy in early_copies:
-        copy.start()
     tokens_copy.start()
-    pool_copy.start()
-
+    early_copies[2].start()
     barrier = pltpu.get_barrier_semaphore()
 
     def greet(d, carry):
@@ -390,8 +387,10 @@
             barrier, inc=1, device_id=(ep, peer_high(k) * 2 + lo), device_id_type=MESH
         )
     pl.semaphore_signal(barrier, inc=1, device_id=(ep, hi * 2 + other), device_id_type=MESH)
-    for copy in mixer_copies + weight_copies:
+    for copy in early_copies[:2]:
         copy.start()
+    pool_copy.start()
+
 
     expert_id = lax.broadcasted_iota(jnp.int32, (experts, tok_dev), 0)
     first_slot = (
@@ -418,9 +417,10 @@
             slot_rows[base + k : base + k + 1, :] = slot.astype(jnp.int32)
         return found
 
-    for copy in early_copies:
-        copy.wait()
+    early_copies[2].wait()
     tokens_copy.wait()
+    for copy in mixer_copies + weight_copies:
+        copy.start()
     normed[...] = rms_scale(tokens[...].astype(F32), in_gain[...]).astype(BF16)
     pool_copy.wait()
     pl.semaphore_wait(barrier, ep_size - 1 + highs)
@@ -431,16 +431,6 @@
     @pl.when(ep < ep_size - 1)
     def _():
         send_history.start()
-
-    slot_list = find_slots(tp, 0)
-    own_weights = route_weights[:, tokens_of(tp)]
-    stacked = jnp.concatenate(
-        slot_list
-        + [own_weights[k : k + 1, :] for k in range(top_count)]
-        + [jnp.zeros((columns_of.shape[1] - 2 * top_count, tok_dev), F32)],
-        axis=0,
-    )
-    columns_of[...] = stacked.T
 
     def routed_rows(owner, base, source):
         slot_id = lax.broadcasted_iota(jnp.int32, (rows, tok_dev), 0) + owner * rows
@@ -525,8 +515,9 @@
             lax.fori_loop(1, NEAR, send_near, 0)
             arrived[0, peer_high(k) * 2 + lo] = routed_rows(ep, base, source)
 
-    arrived[0, tp] = routed_rows(ep, 0, normed)
-    stage_a(jnp.int32(0))
+    for copy in early_copies[:2]:
+        copy.wait()
+    slot_list = find_slots(tp, 0)
 
     def send_out(i, carry):
         d = sent_at(i)
@@ -536,6 +527,16 @@
         return carry
 
     lax.fori_loop(0, ep_size - 1, send_out, 0)
+    arrived[0, tp] = routed_rows(ep, 0, normed)
+    stage_a(jnp.int32(0))
+    own_weights = route_weights[:, tokens_of(tp)]
+    stacked = jnp.concatenate(
+        slot_list
+        + [own_weights[k : k + 1, :] for k in range(top_count)]
+        + [jnp.zeros((columns_of.shape[1] - 2 * top_count, tok_dev), F32)],
+        axis=0,
+    )
+    columns_of[...] = stacked.T
 
     def gather_next(d):
         dispatch(d).wait_recv()

time: 133 us -> 133 us (level)
  no operation moved by 1% of the time
where the time goes in v5:
time: 133 us
  Pallas kernels  130 us (98%)
  local copies, waits for them, and re-layouts  1.77 us (1%)
    pallas_call x1, Pallas kernels, on_device(): pl.pallas_call(functools.partial(fused_kernel, capacity), out_shape=(pltp...  130 us

profile of v5, /device:TPU:0, one launch (start us, length us, event | category | flops | bytes accessed | tf_op | source)
XLA Modules:
  0.0 132.8 jit_solution(14795734084248465684)
XLA Ops:
  0.6 130.4 %shard_map.140 = (bf16[128,2048]{1,0:T(8,128)(2,1)S(1)}, bf16[256,2048]{1,0:T(8,128)(2,1)S(1)}) custom-call(bf16[512,256]{1,0:T(8,128)(2,1)} %pool_hbm.1, bf16[1,256,256]{2,1,0:T(8,128)(2,1)} %group_hbm.1, f32[1,256]{1,0:T(1,128)} %bitcast.11, bf16[256,2048]{1,0:T(8,128)(2,1)} %out_w_hbm.1, f32[1,2048]{1,0:T(1,128)} %bitcast.6, ...), custom_call_target="tpu_custom_call" | custom-call | flops 16106127360 | bytes 4194304 | tf_op jit(solution)/shard_map/pallas_call | solution.py:813
  131.1 0.8 copy.17
  131.9 1.0 copy.18

commit v6 on v5

--- a/solution.py
+++ b/solution.py
@@ -627,12 +627,16 @@
     def reduce(d):
         reduce_core_all(d).wait_recv()
         reduce_core_all(d).wait_send()
-        for high in range(highs):
+
+        def chip_total(high):
             core_in[d, high] = (
                 part[high * 2 + lo].astype(F32) + core_in[d, high].astype(F32)
             ).astype(BF16)
+
         for k in range(1, highs):
+            chip_total(peer_high(k))
             reduce_cross(d, k).start()
+        chip_total(hi)
 
     def send_home(d):
         total = core_in[d, hi].astype(F32)

time: 133 us -> 132 us (level)
  no operation moved by 1% of the time
where the time goes in v6:
time: 132 us
  Pallas kernels  130 us (98%)
  local copies, waits for them, and re-layouts  1.77 us (1%)
    pallas_call x1, Pallas kernels, on_device(): pl.pallas_call(functools.partial(fused_kernel, capacity), out_shape=(pltp...  130 us

profile of v6, /device:TPU:0, one launch (start us, length us, event | category | flops | bytes accessed | tf_op | source)
XLA Modules:
  0.0 132.1 jit_solution(8598834161437170540)
XLA Ops:
  0.6 129.7 %shard_map.140 = (bf16[128,2048]{1,0:T(8,128)(2,1)S(1)}, bf16[256,2048]{1,0:T(8,128)(2,1)S(1)}) custom-call(bf16[512,256]{1,0:T(8,128)(2,1)} %pool_hbm.1, bf16[1,256,256]{2,1,0:T(8,128)(2,1)} %group_hbm.1, f32[1,256]{1,0:T(1,128)} %bitcast.11, bf16[256,2048]{1,0:T(8,128)(2,1)} %out_w_hbm.1, f32[1,2048]{1,0:T(1,128)} %bitcast.6, ...), custom_call_target="tpu_custom_call" | custom-call | flops 16106127360 | bytes 4194304 | tf_op jit(solution)/shard_map/pallas_call | solution.py:817
  130.4 0.8 copy.17
  131.2 1.0 copy.18

commit v7 on v6

--- a/solution.py
+++ b/solution.py
@@ -233,7 +233,7 @@
             part.at[high * 2 + other],
             core_in.at[d, high],
             c2_send.at[0],
-            c2_recv.at[d],
+            c2_recv.at[d, high],
             ep,
             hi * 2 + other,
         )
@@ -243,7 +243,7 @@
             part.at[0:highs],
             core_in.at[d],
             c2_send.at[0],
-            c2_recv.at[d],
+            c2_recv.at[d, 0],
             ep,
             hi * 2 + other,
         )
@@ -621,14 +621,13 @@
     def compute(d):
         gather_core_in(d).wait_recv()
         experts_on(d)
-        for high in range(highs):
-            reduce_core(d, high).start()
+        for k in range(1, highs):
+            reduce_core(d, peer_high(k)).start()
+        reduce_core(d, hi).start()
 
     def reduce(d):
-        reduce_core_all(d).wait_recv()
-        reduce_core_all(d).wait_send()
-
         def chip_total(high):
+            reduce_core(d, high).wait_recv()
             core_in[d, high] = (
                 part[high * 2 + lo].astype(F32) + core_in[d, high].astype(F32)
             ).astype(BF16)
@@ -637,6 +636,7 @@
             chip_total(peer_high(k))
             reduce_cross(d, k).start()
         chip_total(hi)
+        reduce_core_all(d).wait_send()
 
     def send_home(d):
         total = core_in[d, hi].astype(F32)
@@ -799,7 +799,7 @@
         dma((1,)),
         dma((ep_size,)),
         dma((1,)),
-        dma((ep_size,)),
+        dma((ep_size, highs)),
         dma((highs - 1,)),
         dma((ep_size, highs - 1)),
         dma((1,)),

time: 132 us -> 131 us (level)
  Pallas kernels: 130 us -> 128 us
    pallas_call x1, Pallas kernels: 130 us -> 128 us  [on_device(): pl.pallas_call(functools.partial(fused_kernel, capacity), out_shape=(pltp...]
where the time goes in v7:
time: 131 us; the launch traced here: 130 us
  Pallas kernels  128 us (98%)
  local copies, waits for them, and re-layouts  1.77 us (1%)
    pallas_call x1, Pallas kernels, on_device(): pl.pallas_call(functools.partial(fused_kernel, capacity), out_shape=(pltp...  128 us

profile of v7, /device:TPU:0, one launch (start us, length us, event | category | flops | bytes accessed | tf_op | source)
XLA Modules:
  0.0 130.4 jit_solution(3062064592416943017)
XLA Ops:
  0.6 128.0 %shard_map.140 = (bf16[128,2048]{1,0:T(8,128)(2,1)S(1)}, bf16[256,2048]{1,0:T(8,128)(2,1)S(1)}) custom-call(bf16[512,256]{1,0:T(8,128)(2,1)} %pool_hbm.1, bf16[1,256,256]{2,1,0:T(8,128)(2,1)} %group_hbm.1, f32[1,256]{1,0:T(1,128)} %bitcast.11, bf16[256,2048]{1,0:T(8,128)(2,1)} %out_w_hbm.1, f32[1,2048]{1,0:T(1,128)} %bitcast.6, ...), custom_call_target="tpu_custom_call" | custom-call | flops 16106127360 | bytes 4194304 | tf_op jit(solution)/shard_map/pallas_call | solution.py:817
  128.6 0.8 copy.17
  129.4 1.0 copy.18
